TPU v7x, 512 devices: a 4x2x32 block of a 4x8x32 slice. The times are simulated.
512 devices in a mesh: grp: 2 (over y), kv: 64 (over z, core), tp: 4 (over x).
Axes of the slice: x: 4, y: 2, z: 32, core: 2. Of those that a mesh axis runs over, the one named last changes fastest.
The devices are a block of a 4x8x32 slice.
Arguments:
- tokens: bfloat16 [128, 3, 4096], P(('grp', 'kv')), parts along dimension 0, may hold values from -6 to 6
- input_norm_scale: float32 [4096], replicated, may hold values from 0.1 to 1.9
- head_input_matrix: bfloat16 [4096, 8192], P('kv', 'tp'), may hold values from -0.09375 to 0.09375
- output_gate_matrix: bfloat16 [4096, 8192], P('kv', 'tp'), may hold values from -0.09375 to 0.09375
- group_input_matrix: bfloat16 [4096, 512], P('kv', 'tp'), may hold values from -0.09375 to 0.09375
- group_readout_matrix: bfloat16 [4096, 512], P('kv', 'tp'), may hold values from -0.09375 to 0.09375
- step_size_matrix: bfloat16 [4096, 128], P(None, 'tp'), may hold values from -0.09375 to 0.09375
- step_size_bias: float32 [128], P('tp'), may hold values from -4 to -1
- log_decay_rate: float32 [128], P('tp'), may hold values from -4.6 to 2
- direct_path_weight: float32 [128], P('tp'), may hold values from 0.1 to 1.9
- convolution_tap_weight: bfloat16 [4, 8, 1152], P(None, 'tp'), may hold values from -3 to 3
- convolution_history_rows: bfloat16 [128, 6, 8, 1152], P(('grp', 'kv'), None, 'tp'), parts along dimension 0, may hold values from -6 to 6
- per_proposal_states: float32 [128, 3, 128, 64, 64], P(('grp', 'kv'), None, 'tp'), parts along dimension 0, may hold values from -4 to 4
- accepted: int32 [128], P(('grp', 'kv')), parts along dimension 0, may hold values from 1 to 3
- proposal_extra_decay: float32 [128, 3, 128], P(('grp', 'kv'), None, 'tp'), parts along dimension 0, may hold values from -0.69 to 0
- group_norm_scale: float32 [8192], P('tp'), may hold values from 0.1 to 1.9
- output_projection_matrix: bfloat16 [8192, 4096], P('tp', 'kv'), may hold values from -0.0625 to 0.0625
Outputs:
- mixed: bfloat16 [128, 3, 4096], P(('grp', 'tp'), None, 'kv'), parts along dimension 0
- new_states: float32 [128, 3, 128, 64, 64], P(('grp', 'kv'), None, 'tp'), parts along dimension 0
- new_tail: bfloat16 [128, 6, 8, 1152], P(('grp', 'kv'), None, 'tp'), parts along dimension 0
There are 2 independent parts, one for each index of `grp`. A program takes and returns all parts, laid end to end along the dimension named above; an argument that names none is the same for every part. Nothing has to cross between parts.
All inputs are finite; a program needn't handle non-finite values.
Results may differ from a plain program's by a relative error of at most 0.015.
Values may be sent and summed in bfloat16 or wider, within the bound.
A program may use at most 64 MiB of HBM per device.

v0:
```python
import jax
import jax.numpy as jnp
from jax import lax
from jax.sharding import Mesh
from jax.sharding import PartitionSpec as P

KV = ("kv_0", "kv_1")
GRP_KV = ("grp", "kv_0", "kv_1")


epsilon = 1e-06


def in_blocks(x, dim, size):
    lengths = x.shape
    parts = x.reshape(*lengths[:dim], size, lengths[dim] // size, *lengths[dim + 1 :])
    return jnp.moveaxis(parts, dim, 0)


def in_order(parts, dim):
    parts = jnp.moveaxis(parts, 0, dim)
    lengths = parts.shape
    return parts.reshape(*lengths[:dim], lengths[dim] * lengths[dim + 1], *lengths[dim + 2 :])


def exchange_in_order(parts, axes, turns):
    lengths = [lax.axis_size(a) for a in axes]
    parts = parts.reshape(*lengths, *parts.shape[1:])
    for k in turns:
        parts = lax.all_to_all(parts, axes[k], split_axis=k, concat_axis=k, tiled=True)
    return parts.reshape(-1, *parts.shape[len(axes) :])


def two_step_exchange(x, groups, turns, split_dim, concat_dim):
    size = lax.axis_size(groups[0]) * lax.axis_size(groups[1])
    parts = in_blocks(x, split_dim, size)
    return in_order(exchange_in_order(parts, groups, turns), concat_dim)


def reduced_to_own(parts, axes, turns):
    inside = parts.shape[1:]
    parts = parts.reshape(*(lax.axis_size(a) for a in axes), *inside)
    parts = jnp.moveaxis(parts, turns, range(len(axes))).reshape(-1, *inside)
    for k in turns:
        parts = lax.psum_scatter(parts, axes[k], scatter_dimension=0, tiled=True)
    return parts[0]


def sum_by_axis(x, axes, turns, dim):
    size = lax.axis_size(axes)
    return reduced_to_own(in_blocks(x, dim, size), axes, turns)


def gather_in_order(x, axes, turns):
    parts = x[None]
    for k in turns:
        parts = lax.all_gather(parts, axes[k], axis=0, tiled=True)
    carried = [lax.axis_size(axes[k]) for k in reversed(turns)]
    parts = parts.reshape(*carried, *x.shape)
    turned = sorted(range(len(turns)), key=lambda place: turns[len(turns) - 1 - place])
    return parts.transpose(*turned, *range(len(turns), parts.ndim)).reshape(-1, *x.shape)


def gather_axes(x, axes, turns, dim):
    return in_order(gather_in_order(x, axes, turns), dim)


def sum_at_owner(x, axis, dim):
    size = lax.axis_size(axis)
    parts = lax.all_to_all(in_blocks(x, dim, size), axis, 0, 0, tiled=True)
    return jnp.sum(parts.astype(jnp.float32), axis=0)


def rms_scale(values):
    return lax.rsqrt(jnp.mean(values * values, axis=-1, keepdims=True) + epsilon)


def causal_states(log_decay_factor, head_step_size, ssm_inputs, inject, start_state):
    cumulative = jnp.cumsum(log_decay_factor, axis=1)
    length = log_decay_factor.shape[1]
    lower = (jnp.arange(length)[:, None] >= jnp.arange(length)[None, :])[None, :, :, None]
    spread = cumulative[:, :, None, :] - cumulative[:, None, :, :]
    factors = jnp.where(lower, jnp.exp(jnp.where(lower, spread, 0.0)), 0.0)
    mixing = factors * head_step_size[:, None, :, :]
    carried = jnp.exp(cumulative)[..., None, None] * start_state[:, None]
    return carried + jnp.einsum("sjih,sihp,sihn->sjhpn", mixing, ssm_inputs, inject)


def combine_head_outputs(
    incoming_token_rows,
    gate_portion,
    unactivated_step,
    step_size_bias,
    log_decay_rate,
    direct_path_weight,
    convolution_tap_weight,
    convolution_history_rows,
    per_proposal_states,
    accepted,
    proposal_extra_decay,
    group_norm_scale,
):
    sequences, proposals, group_count, group_width = incoming_token_rows.shape
    head_count = step_size_bias.shape[0]
    head_dim = per_proposal_states.shape[3]
    state_size = per_proposal_states.shape[4]
    per_group = head_count // group_count
    group_inner = per_group * head_dim
    tap_count = convolution_tap_weight.shape[0]
    offsets = accepted[:, None] + jnp.arange(tap_count - 1, dtype=jnp.int32)[None, :]
    context = jnp.take_along_axis(convolution_history_rows, offsets[:, :, None, None], axis=1)
    convolution_span = jnp.concatenate([context, incoming_token_rows], axis=1)
    widened = convolution_span.astype(jnp.float32)
    convolved = jnp.zeros((sequences, proposals, group_count, group_width), jnp.float32)
    for conv_tap in range(tap_count):
        convolved = convolved + widened[
            :, conv_tap : conv_tap + proposals
        ] * convolution_tap_weight[conv_tap].astype(jnp.float32)
    activated = jax.nn.silu(convolved)
    ssm_inputs = activated[..., :group_inner].reshape(sequences, proposals, head_count, head_dim)
    inject = jnp.repeat(activated[..., group_inner : group_inner + state_size], per_group, axis=2)
    readout = jnp.repeat(activated[..., group_inner + state_size :], per_group, axis=2)
    head_step_size = jax.nn.softplus(unactivated_step + step_size_bias)
    log_decay_factor = proposal_extra_decay - jnp.exp(log_decay_rate) * head_step_size
    chosen = (accepted - 1)[:, None, None, None, None]
    start_state = jnp.take_along_axis(per_proposal_states, chosen, axis=1)[:, 0]
    running_state_rows = causal_states(
        log_decay_factor, head_step_size, ssm_inputs, inject, start_state
    )
    response = (
        jnp.einsum("sjhn,sjhpn->sjhp", readout, running_state_rows)
        + direct_path_weight[:, None] * ssm_inputs
    )
    gate_raw = gate_portion.astype(jnp.float32).reshape(sequences, proposals, head_count, head_dim)
    gate_applied_output = (response * jax.nn.silu(gate_raw)).reshape(
        sequences, proposals, group_count, group_inner
    )
    scaled = (
        gate_applied_output
        * rms_scale(gate_applied_output)
        * group_norm_scale.reshape(group_count, group_inner)
    )
    flat_gated = scaled.astype(jnp.bfloat16).reshape(sequences, proposals, head_count * head_dim)
    return (flat_gated, running_state_rows, convolution_span)


def local(
    tokens,
    input_norm_scale,
    head_input_matrix,
    output_gate_matrix,
    group_input_matrix,
    group_readout_matrix,
    step_size_matrix,
    step_size_bias,
    log_decay_rate,
    direct_path_weight,
    convolution_tap_weight,
    convolution_history_rows,
    per_proposal_states,
    accepted,
    proposal_extra_decay,
    group_norm_scale,
    output_projection_matrix,
):
    local_seqs, proposals, width = tokens.shape
    head_local = step_size_bias.shape[0]
    group_local = convolution_tap_weight.shape[1]
    head_dim = per_proposal_states.shape[3]
    state_size = per_proposal_states.shape[4]
    group_inner = head_local // group_local * head_dim
    widened = tokens.astype(jnp.float32)
    normed = (widened * rms_scale(widened) * input_norm_scale).astype(jnp.bfloat16)
    unactivated_step = jnp.einsum(
        "sjd,dh->sjh", normed, step_size_matrix, preferred_element_type=jnp.float32
    )
    pieces = two_step_exchange(normed, ("kv_0", "kv_1"), (1, 0), 2, 0)
    joined = jnp.concatenate(
        [head_input_matrix, group_input_matrix, group_readout_matrix, output_gate_matrix], axis=1
    )
    summed = sum_by_axis(
        jnp.einsum("sjd,dc->sjc", pieces, joined, preferred_element_type=jnp.float32), KV, (1, 0), 0
    )
    projected = summed.astype(jnp.bfloat16)
    input_width = head_local * head_dim
    inject_width = group_local * state_size
    part_input = projected[..., :input_width].reshape(
        local_seqs, proposals, group_local, group_inner
    )
    part_inject = projected[..., input_width : input_width + inject_width].reshape(
        local_seqs, proposals, group_local, state_size
    )
    part_readout = projected[
        ..., input_width + inject_width : input_width + 2 * inject_width
    ].reshape(local_seqs, proposals, group_local, state_size)
    gate_portion = projected[..., input_width + 2 * inject_width :]
    incoming_token_rows = jnp.concatenate([part_input, part_inject, part_readout], axis=-1)
    gate_applied_output, running_state_rows, convolution_span = combine_head_outputs(
        incoming_token_rows,
        gate_portion,
        unactivated_step,
        step_size_bias,
        log_decay_rate,
        direct_path_weight,
        convolution_tap_weight,
        convolution_history_rows,
        per_proposal_states,
        accepted,
        proposal_extra_decay,
        group_norm_scale,
    )
    terms = jnp.einsum(
        "sjc,cd->sjd",
        gather_axes(gate_applied_output, KV, (0, 1), 0),
        output_projection_matrix,
        preferred_element_type=jnp.float32,
    )
    mixed = sum_at_owner(terms.astype(jnp.bfloat16), "tp", 0).astype(jnp.bfloat16)
    return (mixed, running_state_rows, convolution_span)


def solution(mesh):
    finer = Mesh(
        mesh.devices.reshape(mesh.shape["grp"], 32, 2, mesh.shape["tp"]),
        ("grp", "kv_0", "kv_1", "tp"),
    )
    return jax.shard_map(
        local,
        mesh=finer,
        in_specs=(
            P(GRP_KV, None, None),
            P(),
            P(KV, "tp"),
            P(KV, "tp"),
            P(KV, "tp"),
            P(KV, "tp"),
            P(None, "tp"),
            P("tp"),
            P("tp"),
            P("tp"),
            P(None, "tp", None),
            P(GRP_KV, None, "tp", None),
            P(GRP_KV, None, "tp", None, None),
            P(GRP_KV),
            P(GRP_KV, None, "tp"),
            P("tp"),
            P("tp", KV),
        ),
        out_specs=(
            P(("grp", "tp"), None, KV),
            P(GRP_KV, None, "tp", None, None),
            P(GRP_KV, None, "tp", None),
        ),
        check_vma=False,
    )
```

profile of v0, /device:TPU:33, one launch (start us, length us, event | category | flops | bytes accessed | tf_op | source)
XLA Modules:
  0.0 318.1 jit_solution(2151247218022713193)
XLA Ops:
  7.3 0.9 fusion.13
  8.2 0.9 fusion.15
  9.3 44.8 %all_to_all.15 = bf16[2,2,3072]{2,1,0:T(2,128)(2,1)S(1)} all-to-all(bf16[2,2,3072]{2,1,0:T(2,128)(2,1)S(1)} %reshape.473), channel_id=1, replica_groups=mesh['grp'=2,'kv_0'=32,'kv_1'=2,'tp'=4] {'kv_1'}, dimensions={0} | all-to-all | bytes 49152 | tf_op jit(solution)/shard_map/all_to_all | solution.py:30
  54.3 26.6 %all_to_all.16 = bf16[32,2,192]{2,1,0:T(2,128)(2,1)S(1)} all-to-all(bf16[32,2,192]{2,1,0:T(2,128)(2,1)S(1)} %reshape.475), channel_id=1, replica_groups=mesh['grp'=2,'kv_0'=32,'kv_1'=2,'tp'=4] {'kv_0'}, dimensions={0} | all-to-all | bytes 49152 | tf_op jit(solution)/shard_map/all_to_all | solution.py:30
  81.1 1.6 convolution_bitcast_fusion
  82.7 1.9 copy.70
  86.8 1.3 dynamic-slice.4
  88.7 2.3 fusion.2
  91.4 8.8 %reduce-scatter.3.cloned.1.call-done = f32[32,1,3,4352]{3,0,2,1:T(8,128)} async-done(((f32[64,1,3,4352]{3,0,2,1:T(8,128)}), f32[32,1,3,4352]{3,0,2,1:T(8,128)}) %reduce-scatter.3.cloned.1.call-update) | async-done | bytes 1671184 | tf_op jit(solution)/shard_map/reduce_scatter | solution.py:45
  100.2 103.7 %all-reduce.2 = bf16[32,1,3,4352]{3,0,2,1:T(8,128)(2,1)S(1)} all-reduce(f32[32,1,3,4352]{3,0,2,1:T(8,128)} %reduce-scatter.3.cloned.1.call-done), channel_id=3, replica_groups=mesh['grp'=2,'kv_0'=32,'kv_1'=2,'tp'=4] {'kv_0'}, use_global_device_ids=true, to_apply=%region_2.0.clone | all-reduce | flops 417792 | bytes 2506752
  203.9 0.7 dynamic-slice_convert_fusion
  205.0 0.7 pad_maximum_fusion
  205.8 0.7 reshape.445
  206.7 2.7 bitcast_add_fusion
  209.4 0.9 fusion
  210.9 42.2 %all_gather.6 = bf16[32,1,3,2048]{3,2,1,0:T(4,128)(2,1)S(1)} all-gather(bf16[1,1,3,2048]{3,2,1,0:T(4,128)(2,1)S(1)} %multiply_convert_fusion), channel_id=1, replica_groups=mesh['grp'=2,'kv_0'=32,'kv_1'=2,'tp'=4] {'kv_0'}, dimensions={0}, use_global_device_ids=true | all-gather | bytes 405504 | tf_op jit(solution)/shard_map/all_gather | solution.py:57
  253.4 42.1 %all_gather.7 = bf16[64,1,3,2048]{3,0,2,1:T(8,128)(2,1)S(1)} all-gather(bf16[32,1,3,2048]{3,0,2,1:T(8,128)(2,1)S(1)} %copy.78), channel_id=1, replica_groups=mesh['grp'=2,'kv_0'=32,'kv_1'=2,'tp'=4] {'kv_1'}, dimensions={0}, use_global_device_ids=true | all-gather | bytes 1179648 | tf_op jit(solution)/shard_map/all_gather | solution.py:57
  295.5 1.7 copy.79
  297.1 3.0 reshape_reshape.2
  300.1 1.5 convolution_convert_fusion
  301.6 0.7 reshape.477
  302.3 4.0 %all-to-all-start.2 = ((bf16[4,2,1536]{2,1,0:T(2,128)(2,1)}), bf16[4,2,1536]{2,1,0:T(2,128)(2,1)S(1)}, u32[]{:S(2)}, u32[]{:S(2)}) async-start(bf16[4,2,1536]{2,1,0:T(2,128)(2,1)} %reshape.477), calls=%async_computation.3 | async-start | bytes 49152 | tf_op jit(solution)/shard_map/all_to_all | solution.py:70
  306.3 1.9 copy.81
  308.1 2.4 all-to-all-done.2
  (75 shorter events, 5.3 us)
Async XLA Ops:
  7.2 292.9 %copy-start = (bf16[2048,64]{0,1:T(8,128)(2,1)S(1)}, bf16[2048,64]{0,1:T(8,128)(2,1)}, u32[]{:S(2)}) copy-start(bf16[2048,64]{0,1:T(8,128)(2,1)} %param.33) | copy-start | bytes 786436
  7.2 93.0 %reduce-scatter.3.cloned.1.call-start = ((), (), s32[]{:S(2)}) async-start(), calls=%async_computation.4 | async-start | bytes 5013504 | tf_op jit(solution)/shard_map/reduce_scatter | solution.py:45
  84.7 0.7 copy-start.8
  84.7 1.0 copy-start.7
  84.7 1.0 copy-start.9
  84.7 1.2 copy-start.5
  84.7 3.4 %copy-start.4 = (bf16[1,6,2,1152]{3,2,1,0:T(2,128)(2,1)S(1)}, bf16[1,6,2,1152]{3,2,1,0:T(2,128)(2,1)}, u32[]{:S(2)}) copy-start(bf16[1,6,2,1152]{3,2,1,0:T(2,128)(2,1)} %param.28) | copy-start | bytes 82948
  84.7 6.7 %copy-start.2 = (bf16[4,2,1152]{2,1,0:T(2,128)(2,1)S(1)}, bf16[4,2,1152]{2,1,0:T(2,128)(2,1)}, u32[]{:S(2)}) copy-start(bf16[4,2,1152]{2,1,0:T(2,128)(2,1)} %param.27) | copy-start | bytes 55300
  206.7 3.6 %copy-start.1 = (f32[3,32,64]{2,1,0:T(8,128)S(1)}, f32[3,32,64]{2,1,0:T(8,128)}, u32[]{:S(2)}) copy-start(f32[3,32,64]{2,1,0:T(8,128)} %reshape.445) | copy-start | bytes 73732
  206.7 3.6 %copy-start.6 = (f32[32]{0:T(128)S(1)}, f32[32]{0:T(128)}, u32[]{:S(2)}) copy-start(f32[32]{0:T(128)} %param.26) | copy-start | bytes 388
  206.7 4.2 %copy-start.3 = (f32[2048]{0:T(1024)S(1)}, f32[2048]{0:T(1024)}, u32[]{:S(2)}) copy-start(f32[2048]{0:T(1024)} %param.32) | copy-start | bytes 24580
  302.3 8.2 %all-to-all-start.2 = ((bf16[4,2,1536]{2,1,0:T(2,128)(2,1)}), bf16[4,2,1536]{2,1,0:T(2,128)(2,1)S(1)}, u32[]{:S(2)}, u32[]{:S(2)}) async-start(bf16[4,2,1536]{2,1,0:T(2,128)(2,1)} %reshape.477), calls=%async_computation.3 | async-start | bytes 49152 | tf_op jit(solution)/shard_map/all_to_all | solution.py:70
Sparse Core Ops, SparseCore 0:
  84.9 15.2 reduce-scatter.2
where the time goes:
time: 319 us; the launch traced here: 318 us
  blocking collectives  259 us (81%)
  local copies, waits for them, and re-layouts  15.4 us (5%)
  between operations  15 us (5%)
  waiting for transfers between devices  11.3 us (4%)
  matrix products  6.86 us (2%)
  other arithmetic  6.1 us (2%)
  starting transfers between devices  4.01 us (1%)
    unnamed x1, blocking collectives  104 us
    all_gather x2, blocking collectives, gather_in_order(): parts = lax.all_gather(parts, axes[k], axis=0, tiled=True)  84.3 us
    all_to_all x2, blocking collectives, exchange_in_order(): lax.all_to_all(parts, axes[k], split_axis=k, concat_axis=k, tiled=True)  71.5 us
    reduce_scatter x1, waiting for transfers between devices, reduced_to_own(): parts = lax.psum_scatter(parts, axes[k], scatter_dimension=0, tiled=True)  8.83 us
  transfers between devices with their start and end apart: 2, of which 2 were waited for; matrix products, arithmetic and copies ran while one was open for 2% of the time, Pallas kernels for 0%

commit v1 on v0

v1 whole, which is shorter than its diff:
```python
import functools

import jax
import jax.numpy as jnp
from jax import lax
from jax.experimental import pallas as pl
from jax.experimental.pallas import tpu as pltpu
from jax.sharding import Mesh
from jax.sharding import PartitionSpec as P

MESH = pl.DeviceIdType.MESH
EPS = 1e-06
F32 = jnp.float32
BF16 = jnp.bfloat16

KV = ("z", "c")
GRP_KV = ("grp", "z", "c")

NZ = 32
BLK = 896
CB = 5
GBLK = 384


def iota(shape, dim):
    return lax.broadcasted_iota(jnp.int32, shape, dim)


def split3(v):
    hi = v.astype(BF16)
    rest = v - hi.astype(F32)
    mid = rest.astype(BF16)
    lo = (rest - mid.astype(F32)).astype(BF16)
    return hi, mid, lo


def dot(a, b):
    return jnp.dot(a, b, preferred_element_type=F32)


def dot_nt(a, b):
    return lax.dot_general(a, b, (((1,), (1,)), ((), ())), preferred_element_type=F32)


def dot_tn(a, b):
    return lax.dot_general(a, b, (((0,), (0,)), ((), ())), preferred_element_type=F32)


def silu(v):
    return v / (1.0 + jnp.exp(-v))


def one_hot(cond):
    return jnp.where(cond, 1.0, 0.0).astype(BF16)


PIECES = (
    (0, 0, 896, 0, 0),
    (0, 896, 896, 1, 0),
    (0, 1792, 256, 2, 0),
    (2, 0, 128, 2, 256),
    (3, 0, 128, 2, 384),
    (1, 0, 384, 2, 512),
    (1, 384, 896, 3, 0),
    (1, 1280, 768, 4, 0),
)


def kernel(
    tok_h, ins_h, wh_h, wg_h, wi_h, wr_h, ws_h, bias_h, ldr_h, dpw_h, tap_h, hist_h, st_h, acc_s, ped_h, gns_h, wo_h,
    mixed_o, states_o, tail_o,
    tok, ins, ws, bias, ldr, dpw, tap, hist, st, ped, gns, wo, wop,
    w2, nst, xs, part, mem, cout, cin, gath, gown, fin, fst, snew, s0cat, span_v,
    lsem, wsend, wrecv, asend, arecv, msend, mrecv, csend, crecv, gsend, grecv, nrecv, fsend, frecv, osem,
):
    z = lax.axis_index("z")
    c = lax.axis_index("c")
    t = lax.axis_index("tp")
    n_tp = lax.axis_size("tp")

    def at(offset):
        return lax.rem(z + (offset + NZ) % NZ, NZ)

    barrier = pltpu.get_barrier_semaphore()

    def greet(k, _):
        pl.semaphore_signal(barrier, inc=1, device_id={"z": lax.rem(z + k, NZ)}, device_id_type=MESH)
        return 0

    lax.fori_loop(1, NZ, greet, 0)
    others = [(dc, dt) for dc in range(2) for dt in range(n_tp) if (dc, dt) != (0, 0)]
    for dc, dt in others:
        pl.semaphore_signal(
            barrier, inc=1, device_id={"c": lax.rem(c + dc, 2), "tp": lax.rem(t + dt, n_tp)}, device_id_type=MESH
        )

    pairs = [
        (tok_h.at[0], tok), (ins_h, ins), (ws_h, ws), (bias_h, bias), (ldr_h, ldr), (dpw_h, dpw), (tap_h, tap),
        (hist_h.at[0], hist), (ped_h.at[0], ped), (gns_h, gns), (st_h, st), (wo_h, wo),
    ]
    loads = [pltpu.make_async_copy(src, dst, lsem.at[i]) for i, (src, dst) in enumerate(pairs)]
    sources = (wh_h, wg_h, wi_h, wr_h)
    mine = pl.multiple_of(c * 64, 64)
    for i, (source, first, count, row, lane) in enumerate(PIECES):
        loads.append(
            pltpu.make_async_copy(
                sources[source].at[:, first : first + count],
                w2.at[pl.ds(pl.multiple_of(row * 128 + mine, 64), 64), lane : lane + count],
                lsem.at[len(pairs) + i],
            )
        )
    for cp in loads:
        cp.start()

    loads[0].wait()
    loads[1].wait()
    wide = tok[...].astype(F32)
    scale = lax.rsqrt(jnp.sum(wide * wide, axis=-1, keepdims=True) * (1.0 / wide.shape[1]) + EPS)
    normed = (wide * scale * ins[...]).astype(BF16)
    row16 = iota((16, 3), 0)
    spread = one_hot((row16 // CB == iota((16, 3), 1)) & (row16 < 3 * CB))
    sent = dot(spread, normed).astype(BF16)
    for k in range(NZ):
        nst[k] = sent[:, k * 128 : (k + 1) * 128]

    pl.semaphore_wait(barrier, NZ - 1 + len(others))

    def send_slice(k, _):
        to = lax.rem(z + k, NZ)
        pltpu.make_async_remote_copy(
            src_ref=nst.at[to], dst_ref=xs.at[z], send_sem=asend, recv_sem=arecv, device_id={"z": to}, device_id_type=MESH
        ).start()
        return 0

    lax.fori_loop(1, NZ, send_slice, 0)
    xs[z] = nst[z]

    partner = {"c": 1 - c}
    shares = []
    for i, (source, first, count, row, lane) in enumerate(PIECES):
        shares.append(
            pltpu.make_async_remote_copy(
                src_ref=sources[source].at[:, first : first + count],
                dst_ref=w2.at[pl.ds(pl.multiple_of(row * 128 + mine, 64), 64), lane : lane + count],
                send_sem=wsend.at[i], recv_sem=wrecv.at[i], device_id=partner, device_id_type=MESH,
            )
        )
    shares.append(
        pltpu.make_async_remote_copy(
            src_ref=wo_h, dst_ref=wop, send_sem=wsend.at[len(PIECES)], recv_sem=wrecv.at[len(PIECES)],
            device_id=partner, device_id_type=MESH,
        )
    )
    for cp in shares:
        cp.start()

    for cp in loads[2:]:
        cp.wait()
    w2[4 * 128 :, 768:] = jnp.zeros((128, 128), BF16)
    step_raw = dot(normed, ws[...])
    raw = step_raw + bias[...]
    step = jnp.maximum(raw, 0.0) + jnp.log1p(jnp.exp(-jnp.abs(raw)))
    decay = ped[...] - jnp.exp(ldr[...]) * step
    cum0 = decay[0:1]
    cum1 = cum0 + decay[1:2]
    cum2 = cum1 + decay[2:3]
    none = jnp.zeros_like(cum0)
    zeros5 = jnp.zeros((5, cum0.shape[1]), F32)

    def rows(a, b, d):
        return jnp.concatenate([a, b, d, zeros5], axis=0)

    per_head = jnp.concatenate(
        [
            rows(jnp.exp(cum0), jnp.exp(cum1), jnp.exp(cum2)),
            rows(step[0:1], step[1:2], step[2:3]),
            rows(none, jnp.exp(cum1 - cum0) * step[0:1], jnp.exp(cum2 - cum1) * step[1:2]),
            rows(none, none, jnp.exp(cum2 - cum0) * step[0:1]),
            rows(dpw[...], dpw[...], dpw[...]),
        ],
        axis=0,
    )
    heads = per_head.shape[1]
    lanes = heads * 64
    to_head = iota((heads, lanes), 1) - iota((heads, lanes), 0) * 64
    expand = one_hot((to_head >= 0) & (to_head < 64))
    hi, mid, lo = split3(per_head)
    wide_heads = dot(hi, expand) + dot(mid, expand) + dot(lo, expand)
    carry_w, mix0, mix1, mix2, direct = (wide_heads[i * 8 : (i + 1) * 8] for i in range(5))

    start = jnp.clip(acc_s[0] - 1, 0, 2)
    ones3 = jnp.ones((3, 64), BF16)
    for g in range(2):
        at_g = slice(g * 1024, (g + 1) * 1024)
        s0 = st[start, at_g, :]
        s_hi = s0.astype(BF16)
        s_lo = (s0 - s_hi.astype(F32)).astype(BF16)
        s0cat[at_g, :] = jnp.concatenate([s_hi, s_lo], axis=1)
        for j in range(3):
            line = carry_w[j : j + 1, at_g]
            l_hi, l_mid, l_lo = split3(line)
            stack = jnp.concatenate([l_hi.astype(F32), l_mid.astype(F32), l_lo.astype(F32)], axis=0).astype(BF16)
            snew[j, at_g, :] = dot_tn(stack, ones3) * s0

    def in_order(v):
        a, b = v[:, 0, :], v[:, 1, :]
        return jnp.concatenate(
            [a[:, :1024], b[:, :1024], a[:, 1024:1088], b[:, 1024:1088], a[:, 1088:], b[:, 1088:]], axis=1
        )

    kept = in_order(hist[...].astype(F32))
    taps = in_order(tap[...].astype(F32))
    accepted = acc_s[0]
    context = jnp.where(accepted == 1, kept[1:4], jnp.where(accepted == 2, kept[2:5], kept[3:6]))
    context = jnp.concatenate([context, jnp.zeros((5, context.shape[1]), F32)], axis=0)

    for cp in shares:
        cp.wait_recv()
    pltpu.make_async_remote_copy(
        src_ref=nst.at[0 : NZ - 1], dst_ref=xs.at[0 : NZ - 1], send_sem=asend, recv_sem=arecv, device_id=partner,
        device_id_type=MESH,
    ).wait_recv()
    x_all = xs[...].reshape(NZ * 16, 128)
    block_of = lax.rem(lax.rem(iota((NZ * 16, 128), 0), 16), CB)
    zero = jnp.zeros_like(x_all)
    stacked = jnp.concatenate([jnp.where(block_of == cb, x_all, zero) for cb in range(CB)], axis=1)
    for n0, n1 in ((0, 256), (256, 512), (512, 768), (768, 896)):
        part[:, :, n0:n1] = dot(stacked, w2[:, n0:n1]).astype(BF16).reshape(NZ, 16, n1 - n0)

    def member(delta, hop, head, slot):
        pltpu.make_async_remote_copy(
            src_ref=part.at[at(delta)], dst_ref=mem.at[head // 4, slot], send_sem=msend, recv_sem=mrecv.at[head // 4],
            device_id={"z": at(hop)}, device_id_type=MESH,
        ).start()

    def members(head):
        member((head + 1) % NZ, 1, head, 0)
        member((head - 1) % NZ, -1, head, 1)
        if head < 16:
            member(head + 2, 2, head, 2)
        if head > 16:
            member(head - 2, -2, head, 2)
        if head == 0:
            member(NZ - 2, -2, head, 3)

    def quad(head):
        count = {0: 4, 16: 2}.get(head, 3)
        pltpu.make_async_remote_copy(
            src_ref=mem.at[head // 4, 0:count], dst_ref=mem.at[head // 4, 0:count], send_sem=msend,
            recv_sem=mrecv.at[head // 4], device_id=partner, device_id_type=MESH,
        ).wait_recv()
        total = part[at(head)].astype(F32)
        for slot in range(count):
            total += mem[head // 4, slot].astype(F32)
        return total

    def chain(step_at, hop):
        return pltpu.make_async_remote_copy(
            src_ref=cout.at[step_at], dst_ref=cin.at[step_at], send_sem=csend.at[step_at], recv_sem=crecv.at[step_at],
            device_id={"z": at(hop)}, device_id_type=MESH,
        )

    right = [chain(i, 4) for i in range(4)]
    left = [chain(4 + i, -4) for i in range(3)]
    for head in (16, 12, 20):
        members(head)
    cout[0] = quad(16).astype(BF16)
    right[0].start()
    cout[4] = quad(20).astype(BF16)
    left[0].start()
    for head in (8, 24):
        members(head)
    total = quad(12)
    right[0].wait_recv()
    cout[1] = (total + cin[0].astype(F32)).astype(BF16)
    right[1].start()
    total = quad(24)
    left[0].wait_recv()
    cout[5] = (total + cin[4].astype(F32)).astype(BF16)
    left[1].start()
    for head in (4, 28):
        members(head)
    total = quad(8)
    right[1].wait_recv()
    cout[2] = (total + cin[1].astype(F32)).astype(BF16)
    right[2].start()
    total = quad(28)
    left[1].wait_recv()
    cout[6] = (total + cin[5].astype(F32)).astype(BF16)
    left[2].start()
    members(0)
    total = quad(4)
    right[2].wait_recv()
    cout[3] = (total + cin[2].astype(F32)).astype(BF16)
    right[3].start()
    total = quad(0)
    left[2].wait_recv()
    total += cin[6].astype(F32)
    right[3].wait_recv()
    total += cin[3].astype(F32)
    owned = total.astype(BF16)

    urow = iota((8 * CB, 16), 0)
    ucol = iota((8 * CB, 16), 1)
    ublk, uj = urow // 8, lax.rem(urow, 8) - 3
    unpack = one_hot((ucol == uj * CB + ublk) & (uj >= 0) & (uj < 3))
    wide_rows = dot(unpack, owned)
    fresh = jnp.concatenate([wide_rows[cb * 8 : (cb + 1) * 8] for cb in range(CB)], axis=1)
    span = fresh[:, :2304] + context
    gate = pltpu.roll(fresh[:, 2304:4352], 5, 0)

    conv = span * taps[0:1]
    for k in range(1, 4):
        conv += pltpu.roll(span, 8 - k, 0) * taps[k : k + 1]
    live = iota(conv.shape, 0) < 3
    act = jnp.where(live, silu(conv), 0.0)
    x = act[:, :2048]
    inject = act[:, 2048:2176]
    readout = act[:, 2176:2304]
    x1 = pltpu.roll(x, 1, 0)
    x2 = pltpu.roll(x, 2, 0)
    i1 = pltpu.roll(inject, 1, 0)
    i2 = pltpu.roll(inject, 2, 0)

    outs = []
    for g in range(2):
        at_g = slice(g * 1024, (g + 1) * 1024)
        half = slice(g * 64, (g + 1) * 64)
        rd = readout[:, half]
        r_hi = rd.astype(BF16)
        r_lo = (rd - r_hi.astype(F32)).astype(BF16)
        both = jnp.concatenate([r_hi, r_hi], axis=1)
        low = jnp.concatenate([r_lo, jnp.zeros_like(r_lo)], axis=1)
        s_part = s0cat[at_g, :]
        first = dot_nt(both, s_part) + dot_nt(low, s_part)
        d0 = jnp.sum(rd * inject[:, half], axis=1, keepdims=True)
        d1 = jnp.sum(rd * i1[:, half], axis=1, keepdims=True)
        d2 = jnp.sum(rd * i2[:, half], axis=1, keepdims=True)
        response = (
            carry_w[:, at_g] * first
            + mix0[:, at_g] * x[:, at_g] * d0
            + mix1[:, at_g] * x1[:, at_g] * d1
            + mix2[:, at_g] * x2[:, at_g] * d2
            + direct[:, at_g] * x[:, at_g]
        )
        gated = jnp.where(live[:, :1024], response * silu(gate[:, at_g]), 0.0)
        norm = lax.rsqrt(jnp.sum(gated * gated, axis=1, keepdims=True) * (1.0 / 1024) + EPS)
        outs.append(gated * norm * gns[:, at_g])
    gated = jnp.concatenate(outs, axis=1)

    stack = jnp.concatenate([gated[:, cb * GBLK : (cb + 1) * GBLK] for cb in range(CB)], axis=0).astype(BF16)
    prow = iota((16, 8 * CB), 0)
    pcol = iota((16, 8 * CB), 1)
    packed = dot(one_hot(prow == lax.rem(pcol, 8) * CB + pcol // 8), stack)
    rest = gated[:, CB * GBLK :]
    last = jnp.concatenate([rest[j : j + 1] for j in range(3)], axis=1)
    packed = jnp.where(iota((16, GBLK), 0) == 15, jnp.broadcast_to(last, (16, GBLK)), packed)
    gown[...] = packed.astype(BF16)
    gath[z] = packed.astype(BF16)

    def share(src_ref, slot, hop, recv):
        pltpu.make_async_remote_copy(
            src_ref=src_ref, dst_ref=gath.at[slot], send_sem=gsend, recv_sem=recv, device_id={"z": at(hop)},
            device_id_type=MESH,
        ).start()

    for k in (4, 3, 5, 2, 6, 1, 7):
        share(gown, z, 4 * k, grecv.at[k])
    for hop in (-2, -1, 1, 2):
        share(gown, z, hop, nrecv)

    for g in range(2):
        at_g = slice(g * 1024, (g + 1) * 1024)
        half = slice(g * 64, (g + 1) * 64)
        b8 = inject[:, half]
        b_hi = b8.astype(BF16).astype(F32)
        b_lo = b8 - b_hi
        rhs = jnp.concatenate([b_hi, b_lo, b_hi], axis=0).astype(BF16)
        live0 = iota((8, 1024), 0)
        for j in range(3):
            coef = jnp.zeros((8, 1024), F32)
            for i in range(j + 1):
                mix = (mix0, mix1, mix2)[j - i]
                coef = jnp.where(live0 == i, mix[j : j + 1, at_g], coef)
            a8 = coef * x[:, at_g]
            a_hi = a8.astype(BF16).astype(F32)
            a_lo = a8 - a_hi
            lhs = jnp.concatenate([a_hi, a_hi, a_lo], axis=0).astype(BF16)
            snew[j, at_g, :] += dot_tn(lhs, rhs)
    span_v[...] = span.astype(BF16)
    stores = [
        pltpu.make_async_copy(snew, states_o, osem.at[0]),
        pltpu.make_async_copy(span_v, tail_o, osem.at[1]),
    ]
    for cp in stores:
        cp.start()

    for k in (1, 7, 2, 6, 3, 5, 4):
        slot = at(-4 * k)
        pltpu.make_async_remote_copy(
            src_ref=gown, dst_ref=gath.at[slot], send_sem=gsend, recv_sem=grecv.at[k], device_id=partner, device_id_type=MESH
        ).wait_recv()
        for hop in (-1, 1) + ((2,) if k < 4 else (-2,) if k > 4 else ()):
            share(gath.at[slot], slot, hop, nrecv)
    pltpu.make_async_remote_copy(
        src_ref=gath.at[0:24], dst_ref=gath.at[0:24], send_sem=gsend, recv_sem=nrecv, device_id=partner, device_id_type=MESH
    ).wait_recv()

    srow = iota((32 * CB, 128), 0)
    scol = iota((32 * CB, 128), 1)
    m, scb = lax.rem(srow, 32), srow // 32
    select = one_hot((m // 4 == scol // 16) & (lax.rem(scol, 16) == lax.rem(m, 4) * CB + scb) & (lax.rem(m, 4) < 3))
    m2 = iota((32, 128), 0)
    c2 = iota((32, 128), 1)
    pick = [one_hot((m2 // 4 == c2 // 16) & (lax.rem(c2, 16) == 15) & (lax.rem(m2, 4) == j)) for j in range(3)]
    inputs = []
    for tb in range(4):
        block = gath[tb * 8 : (tb + 1) * 8].reshape(128, GBLK)
        y = dot(select, block)
        tail = sum(dot(pick[j], block[:, j * 128 : (j + 1) * 128]) for j in range(3))
        inputs.append(jnp.concatenate([y[cb * 32 : (cb + 1) * 32] for cb in range(CB)] + [tail], axis=1).astype(BF16))
    full = jnp.concatenate(inputs, axis=0)
    own_cols = dot(full, wo[...]).astype(BF16)
    partner_cols = dot(full, wop[...]).astype(BF16)
    for tb in range(4):
        fst[0, tb] = own_cols[tb * 32 : (tb + 1) * 32]
        fst[1, tb] = partner_cols[tb * 32 : (tb + 1) * 32]

    finals = []
    for i, (dc, dt) in enumerate(others):
        to = lax.rem(t + dt, n_tp)
        finals.append(
            pltpu.make_async_remote_copy(
                src_ref=fst.at[dc, to], dst_ref=fin.at[c, t], send_sem=fsend.at[i], recv_sem=frecv.at[i],
                device_id={"c": lax.rem(c + dc, 2), "tp": to}, device_id_type=MESH,
            )
        )
    for cp in finals:
        cp.start()
    fin[c, t] = fst[0, t]
    for cp in finals:
        cp.wait_recv()
    for k in range(2):
        total = fin[k, 0].astype(F32)
        for i in range(1, 4):
            total += fin[k, i].astype(F32)
        mixed_o[k] = total.astype(BF16)

    for cp in stores:
        cp.wait()
    for cp in shares:
        cp.wait_send()
    for cp in right + left:
        cp.wait_send()
    for cp in finals:
        cp.wait_send()
    for ref, count, sem in ((xs, NZ - 1, asend), (part, 24, msend), (gath, NZ - 1, gsend)):
        pltpu.make_async_remote_copy(
            src_ref=ref.at[0:count], dst_ref=ref.at[0:count], send_sem=sem, recv_sem=arecv, device_id=partner,
            device_id_type=MESH,
        ).wait_send()


def local(
    tokens,
    input_norm_scale,
    head_input_matrix,
    output_gate_matrix,
    group_input_matrix,
    group_readout_matrix,
    step_size_matrix,
    step_size_bias,
    log_decay_rate,
    direct_path_weight,
    convolution_tap_weight,
    convolution_history_rows,
    per_proposal_states,
    accepted,
    proposal_extra_decay,
    group_norm_scale,
    output_projection_matrix,
):
    width = tokens.shape[2]
    heads = step_size_bias.shape[0]
    channels = heads * 64
    dma = pltpu.SemaphoreType.DMA
    any_space = pl.BlockSpec(memory_space=pl.ANY)
    smem = pl.BlockSpec(memory_space=pltpu.SMEM)
    vmem = pl.BlockSpec(memory_space=pltpu.VMEM)
    mixed, states, tail = pl.pallas_call(
        kernel,
        name="mixer",
        out_shape=(
            jax.ShapeDtypeStruct((2, 32, 64), BF16),
            jax.ShapeDtypeStruct((3, channels, 64), F32),
            jax.ShapeDtypeStruct((8, 2304), BF16),
        ),
        in_specs=[any_space] * 13 + [smem] + [any_space] * 3,
        out_specs=(vmem, any_space, any_space),
        scratch_shapes=[
            pltpu.VMEM((3, width), BF16),
            pltpu.VMEM((1, width), F32),
            pltpu.VMEM((width, heads), BF16),
            pltpu.VMEM((1, heads), F32),
            pltpu.VMEM((1, heads), F32),
            pltpu.VMEM((1, heads), F32),
            pltpu.VMEM((4, 2, 1152), BF16),
            pltpu.VMEM((6, 2, 1152), BF16),
            pltpu.VMEM((3, channels, 64), F32),
            pltpu.VMEM((3, heads), F32),
            pltpu.VMEM((1, channels), F32),
            pltpu.VMEM((channels, 64), BF16),
            pltpu.VMEM((channels, 64), BF16),
            pltpu.VMEM((CB * 128, BLK), BF16),
            pltpu.VMEM((NZ, 16, 128), BF16),
            pltpu.VMEM((NZ, 16, 128), BF16),
            pltpu.VMEM((NZ, 16, BLK), BF16),
            pltpu.VMEM((8, 4, 16, BLK), BF16),
            pltpu.VMEM((7, 16, BLK), BF16),
            pltpu.VMEM((7, 16, BLK), BF16),
            pltpu.VMEM((NZ, 16, GBLK), BF16),
            pltpu.VMEM((16, GBLK), BF16),
            pltpu.VMEM((2, 4, 32, 64), BF16),
            pltpu.VMEM((2, 4, 32, 64), BF16),
            pltpu.VMEM((3, channels, 64), F32),
            pltpu.VMEM((channels, 128), BF16),
            pltpu.VMEM((8, 2304), BF16),
            dma((12 + len(PIECES),)),
            dma((len(PIECES) + 1,)),
            dma((len(PIECES) + 1,)),
            dma,
            dma,
            dma,
            dma((8,)),
            dma((7,)),
            dma((7,)),
            dma,
            dma((8,)),
            dma,
            dma((7,)),
            dma((7,)),
            dma((2,)),
        ],
        compiler_params=pltpu.CompilerParams(
            collective_id=0, has_side_effects=True, vmem_limit_bytes=56 * 1024 * 1024
        ),
    )(
        tokens,
        input_norm_scale.reshape(1, width),
        head_input_matrix,
        output_gate_matrix,
        group_input_matrix,
        group_readout_matrix,
        step_size_matrix,
        step_size_bias.reshape(1, heads),
        log_decay_rate.reshape(1, heads),
        direct_path_weight.reshape(1, heads),
        convolution_tap_weight,
        convolution_history_rows,
        per_proposal_states.reshape(3, channels, 64),
        accepted,
        proposal_extra_decay,
        group_norm_scale.reshape(1, channels),
        output_projection_matrix,
    )
    mixed = mixed.reshape(2, 8, 4, 64)[:, :, :3].transpose(1, 0, 2, 3).reshape(16, 3, 64)
    states = states.reshape(1, 3, heads, 64, 64)
    rows = tail[:6]
    groups = [
        jnp.concatenate(
            [
                rows[:, g * 1024 : (g + 1) * 1024],
                rows[:, 2048 + g * 64 : 2048 + (g + 1) * 64],
                rows[:, 2176 + g * 64 : 2176 + (g + 1) * 64],
            ],
            axis=1,
        )
        for g in range(2)
    ]
    tail = jnp.stack(groups, axis=1)[None]
    return mixed, states, tail


def solution(mesh):
    ring = mesh.shape["kv"] // 2
    assert ring == NZ and mesh.shape["tp"] == 4
    finer = Mesh(
        mesh.devices.reshape(mesh.shape["grp"], ring, 2, mesh.shape["tp"]),
        ("grp", "z", "c", "tp"),
    )
    return jax.shard_map(
        local,
        mesh=finer,
        in_specs=(
            P(GRP_KV, None, None),
            P(),
            P(KV, "tp"),
            P(KV, "tp"),
            P(KV, "tp"),
            P(KV, "tp"),
            P(None, "tp"),
            P("tp"),
            P("tp"),
            P("tp"),
            P(None, "tp", None),
            P(GRP_KV, None, "tp", None),
            P(GRP_KV, None, "tp", None, None),
            P(GRP_KV),
            P(GRP_KV, None, "tp"),
            P("tp"),
            P("tp", KV),
        ),
        out_specs=(
            P(("grp", "tp"), None, KV),
            P(GRP_KV, None, "tp", None, None),
            P(GRP_KV, None, "tp", None),
        ),
        check_vma=False,
    )
```

time: 319 us -> 143 us (0.45)
  blocking collectives: 259 us -> 0 us
  Pallas kernels: 0 us -> 128 us
  between operations: 15 us -> 1.3 us
  waiting for transfers between devices: 11.3 us -> 0 us
  matrix products: 6.86 us -> 0 us
  other arithmetic: 6.1 us -> 0.02 us
  starting transfers between devices: 4.01 us -> 0 us
    pallas_call x0 -> x1, Pallas kernels: none -> 128 us  [local(): pl.pallas_call(kernel, name='mixer', out_shape=(jax.ShapeDtypeStruct((2,...]
    unnamed x1 -> x0, blocking collectives: 104 us -> none
    all_gather x2 -> x0, blocking collectives: 84.3 us -> none  [gather_in_order(): parts = lax.all_gather(parts, axes[k], axis=0, tiled=True)]
    all_to_all x2 -> x0, blocking collectives: 71.5 us -> none  [exchange_in_order(): lax.all_to_all(parts, axes[k], split_axis=k, concat_axis=k, tiled=True)]
    reduce_scatter x1 -> x0, waiting for transfers between devices: 8.83 us -> none  [reduced_to_own(): parts = lax.psum_scatter(parts, axes[k], scatter_dimension=0, tiled=True)]
    dot_general x5 -> x0, matrix products: 6.86 us -> none  [the longest x1 2.66 us: causal_states(): jnp.einsum('sjih,sihp,sihn->sjhpn', mixing, ssm_inputs, inject)]
    unnamed x29 -> x5, local copies, waits for them, and re-layouts: 5.3 us -> 10.1 us
    all_to_all x1 -> x0, starting transfers between devices: 3.95 us -> none  [sum_at_owner(): parts = lax.all_to_all(in_blocks(x, dim, size), axis, 0, 0, tiled=True)]
  transfers between devices with their start and end apart: 2 -> 0, of which waited for: 2 -> 0; matrix products, arithmetic and copies ran while one was open for 2% -> 0% of each run, Pallas kernels for 0% -> 0%
where the time goes in v1:
time: 143 us; the launch traced here: 142 us
  Pallas kernels  128 us (90%)
  local copies, waits for them, and re-layouts  13.2 us (9%)
    pallas_call x1, Pallas kernels, local(): pl.pallas_call(kernel, name='mixer', out_shape=(jax.ShapeDtypeStruct((2,...  128 us
    unnamed x5, local copies, waits for them, and re-layouts  10.1 us

profile of v1, /device:TPU:33, one launch (start us, length us, event | category | flops | bytes accessed | tf_op | source)
XLA Modules:
  0.0 142.1 jit_solution(18361892771875114855)
XLA Ops:
  0.6 2.3 %copy.20.ws_h = bf16[4096,32]{1,0:T(8,128)(2,1)} copy(bf16[4096,32]{0,1:T(8,128)(2,1)} %param.23) | data formatting | bytes 524288 | tf_op args[6]
  2.9 2.0 %copy.22.wo_h = bf16[2048,64]{1,0:T(8,128)(2,1)} copy(bf16[2048,64]{0,1:T(8,128)(2,1)} %param.33) | data formatting | bytes 524288 | tf_op args[16]
  4.8 1.3 copy.21.ped_h
  6.8 127.6 %mixer.1 = (bf16[2,32,64]{2,1,0:T(8,128)(2,1)}, f32[3,2048,64]{2,1,0:T(8,128)}, bf16[8,2304]{1,0:T(8,128)(2,1)}) custom-call(bf16[1,3,4096]{2,1,0:T(4,128)(2,1)} %tok_h.1, f32[1,4096]{1,0:T(1,128)} %bitcast.19, bf16[64,2048]{1,0:T(8,128)(2,1)} %wh_h.1, bf16[64,2048]{1,0:T(8,128)(2,1)} %wg_h.1, bf16[64,128]{1,0:T(8,128)(2,1)} %wi_h.1, bf16[64,128]{1,0:T(8,128)(2,1)} %wr_h.1, ...), custom_call_target="tpu_custom_call" | custom-call | tf_op jit(solution)/shard_map/mixer/pallas_call | solution.py:490
  134.4 0.8 fusion
  135.2 0.7 fusion.1
  136.0 0.1 concatenate.6
  136.1 0.1 concatenate.7
  136.2 0.6 copy.24
  136.8 0.7 slice_bitcast_fusion
  137.5 0.6 copy.23
  138.2 4.0 %copy.27 = f32[1,3,32,64,64]{4,3,2,1,0:T(8,128)} copy(f32[1,3,32,64,64]{4,3,2,1,0:T(8,128)} %bitcast.16) | data formatting | bytes 3145728
  (1 shorter events, 0.0 us)

commit v2 on v1

--- a/solution.py
+++ b/solution.py
@@ -68,10 +68,10 @@
 
 def kernel(
     tok_h, ins_h, wh_h, wg_h, wi_h, wr_h, ws_h, bias_h, ldr_h, dpw_h, tap_h, hist_h, st_h, acc_s, ped_h, gns_h, wo_h,
-    mixed_o, states_o, tail_o,
+    mixed_o, snew, tail_o,
     tok, ins, ws, bias, ldr, dpw, tap, hist, st, ped, gns, wo, wop,
-    w2, nst, xs, part, mem, cout, cin, gath, gown, fin, fst, snew, s0cat, span_v,
-    lsem, wsend, wrecv, asend, arecv, msend, mrecv, csend, crecv, gsend, grecv, nrecv, fsend, frecv, osem,
+    w2, nst, xs, part, mem, cout, cin, gath, gown, fin, fst, s0cat,
+    lsem, wsend, wrecv, asend, arecv, msend, mrecv, csend, crecv, gsend, grecv, nrecv, fsend, frecv,
 ):
     z = lax.axis_index("z")
     c = lax.axis_index("c")
@@ -96,7 +96,7 @@
 
     pairs = [
         (tok_h.at[0], tok), (ins_h, ins), (ws_h, ws), (bias_h, bias), (ldr_h, ldr), (dpw_h, dpw), (tap_h, tap),
-        (hist_h.at[0], hist), (ped_h.at[0], ped), (gns_h, gns), (st_h, st), (wo_h, wo),
+        (hist_h.at[0], hist), (ped_h, ped), (gns_h, gns), (st_h, st), (wo_h, wo),
     ]
     loads = [pltpu.make_async_copy(src, dst, lsem.at[i]) for i, (src, dst) in enumerate(pairs)]
     sources = (wh_h, wg_h, wi_h, wr_h)
@@ -157,13 +157,13 @@
     for cp in loads[2:]:
         cp.wait()
     w2[4 * 128 :, 768:] = jnp.zeros((128, 128), BF16)
-    step_raw = dot(normed, ws[...])
+    step_raw = dot_nt(normed, ws[...])
     raw = step_raw + bias[...]
     step = jnp.maximum(raw, 0.0) + jnp.log1p(jnp.exp(-jnp.abs(raw)))
-    decay = ped[...] - jnp.exp(ldr[...]) * step
-    cum0 = decay[0:1]
-    cum1 = cum0 + decay[1:2]
-    cum2 = cum1 + decay[2:3]
+    decay = jnp.exp(ldr[...]) * step
+    cum0 = ped[0] - decay[0:1]
+    cum1 = cum0 + (ped[1] - decay[1:2])
+    cum2 = cum1 + (ped[2] - decay[2:3])
     none = jnp.zeros_like(cum0)
     zeros5 = jnp.zeros((5, cum0.shape[1]), F32)
 
@@ -387,13 +387,19 @@
             a_lo = a8 - a_hi
             lhs = jnp.concatenate([a_hi, a_hi, a_lo], axis=0).astype(BF16)
             snew[j, at_g, :] += dot_tn(lhs, rhs)
-    span_v[...] = span.astype(BF16)
-    stores = [
-        pltpu.make_async_copy(snew, states_o, osem.at[0]),
-        pltpu.make_async_copy(span_v, tail_o, osem.at[1]),
+    groups = [
+        jnp.concatenate(
+            [
+                span[:, g * 1024 : (g + 1) * 1024],
+                span[:, 2048 + g * 64 : 2048 + (g + 1) * 64],
+                span[:, 2176 + g * 64 : 2176 + (g + 1) * 64],
+            ],
+            axis=1,
+        )
+        for g in range(2)
     ]
-    for cp in stores:
-        cp.start()
+    for i in range(6):
+        tail_o[i] = jnp.concatenate([groups[0][i : i + 1], groups[1][i : i + 1]], axis=0).astype(BF16)
 
     for k in (1, 7, 2, 6, 3, 5, 4):
         slot = at(-4 * k)
@@ -420,8 +426,8 @@
         tail = sum(dot(pick[j], block[:, j * 128 : (j + 1) * 128]) for j in range(3))
         inputs.append(jnp.concatenate([y[cb * 32 : (cb + 1) * 32] for cb in range(CB)] + [tail], axis=1).astype(BF16))
     full = jnp.concatenate(inputs, axis=0)
-    own_cols = dot(full, wo[...]).astype(BF16)
-    partner_cols = dot(full, wop[...]).astype(BF16)
+    own_cols = dot_nt(full, wo[...]).astype(BF16)
+    partner_cols = dot_nt(full, wop[...]).astype(BF16)
     for tb in range(4):
         fst[0, tb] = own_cols[tb * 32 : (tb + 1) * 32]
         fst[1, tb] = partner_cols[tb * 32 : (tb + 1) * 32]
@@ -440,14 +446,19 @@
     fin[c, t] = fst[0, t]
     for cp in finals:
         cp.wait_recv()
+    totals = []
     for k in range(2):
         total = fin[k, 0].astype(F32)
         for i in range(1, 4):
             total += fin[k, i].astype(F32)
-        mixed_o[k] = total.astype(BF16)
-
-    for cp in stores:
-        cp.wait()
+        totals.append(total.astype(BF16))
+    trow = iota((48, 32), 0)
+    tcol = iota((48, 32), 1)
+    want = 4 * (lax.rem(trow, 16) // 2) + trow // 16
+    arranged = sum(dot(one_hot((lax.rem(trow, 2) == k) & (tcol == want)), totals[k]) for k in range(2))
+    for j in range(3):
+        mixed_o[j] = arranged[j * 16 : (j + 1) * 16].astype(BF16)
+
     for cp in shares:
         cp.wait_send()
     for cp in right + left:
@@ -459,6 +470,17 @@
             src_ref=ref.at[0:count], dst_ref=ref.at[0:count], send_sem=sem, recv_sem=arecv, device_id=partner,
             device_id_type=MESH,
         ).wait_send()
+
+
+def store(mixed, states, tail, mixed_o, states_o, tail_o, sem):
+    copies = [
+        pltpu.make_async_copy(src, dst, sem.at[i])
+        for i, (src, dst) in enumerate(((states, states_o), (tail, tail_o), (mixed, mixed_o)))
+    ]
+    for cp in copies:
+        cp.start()
+    for cp in copies:
+        cp.wait()
 
 
 def local(
@@ -491,26 +513,26 @@
         kernel,
         name="mixer",
         out_shape=(
-            jax.ShapeDtypeStruct((2, 32, 64), BF16),
-            jax.ShapeDtypeStruct((3, channels, 64), F32),
-            jax.ShapeDtypeStruct((8, 2304), BF16),
+            pltpu.VMEM((3, 16, 64), BF16),
+            pltpu.VMEM((3, channels, 64), F32),
+            pltpu.VMEM((6, 2, 1152), BF16),
         ),
         in_specs=[any_space] * 13 + [smem] + [any_space] * 3,
-        out_specs=(vmem, any_space, any_space),
+        out_specs=(vmem, vmem, vmem),
         scratch_shapes=[
             pltpu.VMEM((3, width), BF16),
             pltpu.VMEM((1, width), F32),
-            pltpu.VMEM((width, heads), BF16),
+            pltpu.VMEM((heads, width), BF16),
             pltpu.VMEM((1, heads), F32),
             pltpu.VMEM((1, heads), F32),
             pltpu.VMEM((1, heads), F32),
             pltpu.VMEM((4, 2, 1152), BF16),
             pltpu.VMEM((6, 2, 1152), BF16),
             pltpu.VMEM((3, channels, 64), F32),
-            pltpu.VMEM((3, heads), F32),
+            pltpu.VMEM((3, 1, heads), F32),
             pltpu.VMEM((1, channels), F32),
-            pltpu.VMEM((channels, 64), BF16),
-            pltpu.VMEM((channels, 64), BF16),
+            pltpu.VMEM((64, channels), BF16),
+            pltpu.VMEM((64, channels), BF16),
             pltpu.VMEM((CB * 128, BLK), BF16),
             pltpu.VMEM((NZ, 16, 128), BF16),
             pltpu.VMEM((NZ, 16, 128), BF16),
@@ -522,9 +544,7 @@
             pltpu.VMEM((16, GBLK), BF16),
             pltpu.VMEM((2, 4, 32, 64), BF16),
             pltpu.VMEM((2, 4, 32, 64), BF16),
-            pltpu.VMEM((3, channels, 64), F32),
             pltpu.VMEM((channels, 128), BF16),
-            pltpu.VMEM((8, 2304), BF16),
             dma((12 + len(PIECES),)),
             dma((len(PIECES) + 1,)),
             dma((len(PIECES) + 1,)),
@@ -539,7 +559,6 @@
             dma,
             dma((7,)),
             dma((7,)),
-            dma((2,)),
         ],
         compiler_params=pltpu.CompilerParams(
             collective_id=0, has_side_effects=True, vmem_limit_bytes=56 * 1024 * 1024
@@ -551,7 +570,7 @@
         output_gate_matrix,
         group_input_matrix,
         group_readout_matrix,
-        step_size_matrix,
+        step_size_matrix.T,
         step_size_bias.reshape(1, heads),
         log_decay_rate.reshape(1, heads),
         direct_path_weight.reshape(1, heads),
@@ -559,25 +578,25 @@
         convolution_history_rows,
         per_proposal_states.reshape(3, channels, 64),
         accepted,
-        proposal_extra_decay,
+        proposal_extra_decay.transpose(1, 0, 2),
         group_norm_scale.reshape(1, channels),
-        output_projection_matrix,
+        output_projection_matrix.T,
     )
-    mixed = mixed.reshape(2, 8, 4, 64)[:, :, :3].transpose(1, 0, 2, 3).reshape(16, 3, 64)
+    mixed, states, tail = pl.pallas_call(
+        store,
+        name="store",
+        out_shape=(
+            jax.ShapeDtypeStruct((3, 16, 64), BF16),
+            jax.ShapeDtypeStruct((3, channels, 64), F32),
+            jax.ShapeDtypeStruct((6, 2, 1152), BF16),
+        ),
+        in_specs=[pl.BlockSpec(memory_space=pltpu.VMEM)] * 3,
+        out_specs=(any_space,) * 3,
+        scratch_shapes=[dma((3,))],
+    )(*(pltpu.with_memory_space_constraint(v, pltpu.VMEM) for v in (mixed, states, tail)))
+    mixed = mixed.transpose(1, 0, 2)
     states = states.reshape(1, 3, heads, 64, 64)
-    rows = tail[:6]
-    groups = [
-        jnp.concatenate(
-            [
-                rows[:, g * 1024 : (g + 1) * 1024],
-                rows[:, 2048 + g * 64 : 2048 + (g + 1) * 64],
-                rows[:, 2176 + g * 64 : 2176 + (g + 1) * 64],
-            ],
-            axis=1,
-        )
-        for g in range(2)
-    ]
-    tail = jnp.stack(groups, axis=1)[None]
+    tail = tail[None]
     return mixed, states, tail
 
 

time: 143 us -> 130 us (0.909)
  local copies, waits for them, and re-layouts: 13.2 us -> 0 us
    unnamed x5 -> x0, local copies, waits for them, and re-layouts: 10.1 us -> none
    slice x2 -> x0, local copies, waits for them, and re-layouts: 1.57 us -> none  [the longest x1 0.84 us: local(): rows[:, 2176 + g * 64:2176 + (g + 1) * 64]]
    pallas_call x1 -> x2, Pallas kernels: 128 us -> 129 us  [the longest x1 127 us: local(): pl.pallas_call(kernel, name='mixer', out_shape=(pltpu.VMEM((3, 16, 64), B...]
where the time goes in v2:
time: 130 us
  Pallas kernels  129 us (99%)
    pallas_call x1, Pallas kernels, local(): pl.pallas_call(kernel, name='mixer', out_shape=(pltpu.VMEM((3, 16, 64), B...  127 us

profile of v2, /device:TPU:33, one launch (start us, length us, event | category | flops | bytes accessed | tf_op | source)
XLA Modules:
  0.0 130.3 jit_solution(11533381048748825113)
XLA Ops:
  1.3 127.3 %mixer.1 = (bf16[3,16,64]{2,1,0:T(8,128)(2,1)S(1)}, f32[3,2048,64]{2,1,0:T(8,128)S(1)}, bf16[6,2,1152]{2,1,0:T(2,128)(2,1)S(1)}) custom-call(bf16[1,3,4096]{2,1,0:T(4,128)(2,1)} %tok_h.1, f32[1,4096]{1,0:T(1,128)} %bitcast.15, bf16[64,2048]{1,0:T(8,128)(2,1)} %wh_h.1, bf16[64,2048]{1,0:T(8,128)(2,1)} %wg_h.1, bf16[64,128]{1,0:T(8,128)(2,1)} %wi_h.1, ...), custom_call_target="tpu_custom_call" | custom-call | tf_op jit(solution)/shard_map/mixer/pallas_call | solution.py:512
  128.6 1.7 %store.1 = (bf16[3,16,64]{2,1,0:T(8,128)(2,1)}, f32[3,2048,64]{2,1,0:T(8,128)}, bf16[6,2,1152]{2,1,0:T(2,128)(2,1)}) custom-call(bf16[3,16,64]{2,1,0:T(8,128)(2,1)S(1)} %get-tuple-element.9.mixed, f32[3,2048,64]{2,1,0:T(8,128)S(1)} %get-tuple-element.10.states, bf16[6,2,1152]{2,1,0:T(2,128)(2,1)S(1)} %get-tuple-element.11.tail), custom_call_target="tpu_custom_call" | custom-call | tf_op jit(solution)/shard_map/store/pallas_call | solution.py:585

commit v3 on v2

--- a/solution.py
+++ b/solution.py
@@ -71,28 +71,20 @@
     mixed_o, snew, tail_o,
     tok, ins, ws, bias, ldr, dpw, tap, hist, st, ped, gns, wo, wop,
     w2, nst, xs, part, mem, cout, cin, gath, gown, fin, fst, s0cat,
-    lsem, wsend, wrecv, asend, arecv, msend, mrecv, csend, crecv, gsend, grecv, nrecv, fsend, frecv,
+    lsem, wsend, wrecv, asend, arecv, msend, mrecv, csend, crecv, gsend, grecv, nrecv, fsend, frecv, rel0, rel1, r0send, r0recv, r1send, r1recv, may,
 ):
     z = lax.axis_index("z")
     c = lax.axis_index("c")
     t = lax.axis_index("tp")
     n_tp = lax.axis_size("tp")
 
+    o = lax.rem(z + NZ - 1, NZ)
+
     def at(offset):
         return lax.rem(z + (offset + NZ) % NZ, NZ)
 
-    barrier = pltpu.get_barrier_semaphore()
-
-    def greet(k, _):
-        pl.semaphore_signal(barrier, inc=1, device_id={"z": lax.rem(z + k, NZ)}, device_id_type=MESH)
-        return 0
-
-    lax.fori_loop(1, NZ, greet, 0)
-    others = [(dc, dt) for dc in range(2) for dt in range(n_tp) if (dc, dt) != (0, 0)]
-    for dc, dt in others:
-        pl.semaphore_signal(
-            barrier, inc=1, device_id={"c": lax.rem(c + dc, 2), "tp": lax.rem(t + dt, n_tp)}, device_id_type=MESH
-        )
+    def chip(place):
+        return lax.rem(place + 1, NZ)
 
     pairs = [
         (tok_h.at[0], tok), (ins_h, ins), (ws_h, ws), (bias_h, bias), (ldr_h, ldr), (dpw_h, dpw), (tap_h, tap),
@@ -112,27 +104,62 @@
     for cp in loads:
         cp.start()
 
+    barrier = pltpu.get_barrier_semaphore()
+
+    def greet(to, _):
+        pl.semaphore_signal(barrier, inc=1, device_id={"z": chip(to)}, device_id_type=MESH)
+        return 0
+
+    lax.fori_loop(o + 1, NZ, greet, 0)
+    others = [(dc, dt) for dc in range(2) for dt in range(n_tp) if (dc, dt) != (0, 0)]
+    for dc, dt in others:
+        pl.semaphore_signal(
+            barrier, inc=1, device_id={"c": lax.rem(c + dc, 2), "tp": lax.rem(t + dt, n_tp)}, device_id_type=MESH
+        )
+
+    pl.semaphore_wait(barrier, o + len(others))
+
+    def tell(k, _):
+        to = chip(o - k)
+
+        @pl.when((k <= 8) | (k >= 24) | ((k >= 17) & (o < 24)))
+        def _():
+            pl.semaphore_signal(may.at[o], inc=1, device_id={"z": to}, device_id_type=MESH)
+
+        return 0
+
+    lax.fori_loop(1, o + 1, tell, 0)
+
     loads[0].wait()
     loads[1].wait()
     wide = tok[...].astype(F32)
     scale = lax.rsqrt(jnp.sum(wide * wide, axis=-1, keepdims=True) * (1.0 / wide.shape[1]) + EPS)
     normed = (wide * scale * ins[...]).astype(BF16)
-    row16 = iota((16, 3), 0)
-    spread = one_hot((row16 // CB == iota((16, 3), 1)) & (row16 < 3 * CB))
-    sent = dot(spread, normed).astype(BF16)
+    padded = jnp.concatenate([normed.astype(F32), jnp.zeros((1, normed.shape[1]), F32)], axis=0).astype(BF16)
     for k in range(NZ):
-        nst[k] = sent[:, k * 128 : (k + 1) * 128]
-
-    pl.semaphore_wait(barrier, NZ - 1 + len(others))
-
-    def send_slice(k, _):
-        to = lax.rem(z + k, NZ)
-        pltpu.make_async_remote_copy(
-            src_ref=nst.at[to], dst_ref=xs.at[z], send_sem=asend, recv_sem=arecv, device_id={"z": to}, device_id_type=MESH
-        ).start()
+        nst[k] = padded[:, k * 128 : (k + 1) * 128]
+
+    def copy_slice(src_ref, dst_ref, send_sem, recv_sem, to):
+        return pltpu.make_async_remote_copy(
+            src_ref=src_ref, dst_ref=dst_ref, send_sem=send_sem, recv_sem=recv_sem, device_id={"z": chip(to)},
+            device_id_type=MESH,
+        )
+
+    def direct_slice(to):
+        copy_slice(nst.at[chip(to)], xs.at[z], asend, arecv, to).start()
+
+    def send_back(to, _):
+        direct_slice(to)
         return 0
 
-    lax.fori_loop(1, NZ, send_slice, 0)
+    lax.fori_loop(0, o, send_back, 0)
+
+    def send_by_first(to, _):
+        relay = to - 24
+        copy_slice(nst.at[chip(to)], rel1.at[o - relay - 1], asend, r1recv.at[o - relay - 1], relay).start()
+        return 0
+
+    lax.fori_loop(jnp.maximum(o + 17, 24), jnp.minimum(o + 24, NZ), send_by_first, 0)
     xs[z] = nst[z]
 
     partner = {"c": 1 - c}
@@ -214,13 +241,62 @@
     context = jnp.where(accepted == 1, kept[1:4], jnp.where(accepted == 2, kept[2:5], kept[3:6]))
     context = jnp.concatenate([context, jnp.zeros((5, context.shape[1]), F32)], axis=0)
 
+    def send_near(to, _):
+        pl.semaphore_wait(may.at[to], 1)
+        direct_slice(to)
+
+        @pl.when(to + 8 < NZ)
+        def _():
+            slot = o - to + 8
+            copy_slice(nst.at[chip(to + 8)], rel0.at[slot], asend, r0recv.at[slot], to).start()
+
+        return 0
+
+    lax.fori_loop(o + 1, jnp.minimum(o + 9, NZ), send_near, 0)
+
+    def pass_on(rel, slot, source, sems, recv, to):
+        copy_slice(rel.at[slot], rel.at[slot], asend, recv.at[slot], to).wait_recv()
+        copy_slice(rel.at[slot], xs.at[chip(source)], sems.at[slot], arecv, to).start()
+
+    @pl.when(o + 8 < NZ)
+    def _():
+        def pass_right(slot, _):
+            pass_on(rel0, slot, o - 8 + slot, r0send, r0recv, o + 8)
+            return 0
+
+        lax.fori_loop(jnp.maximum(8 - o, 0), 8, pass_right, 0)
+
+    def send_far(to, _):
+        pl.semaphore_wait(may.at[to], 1)
+        direct_slice(to)
+        return 0
+
+    lax.fori_loop(o + 17, 24, send_far, 0)
+
+    @pl.when(o + 24 < NZ)
+    def _():
+        send_far(o + 24, 0)
+
+        def pass_left(slot, _):
+            pass_on(rel1, slot, o + 1 + slot, r1send, r1recv, o + 24)
+            return 0
+
+        lax.fori_loop(0, 7, pass_left, 0)
+
+    lax.fori_loop(o + 25, NZ, send_far, 0)
+
     for cp in shares:
         cp.wait_recv()
     pltpu.make_async_remote_copy(
         src_ref=nst.at[0 : NZ - 1], dst_ref=xs.at[0 : NZ - 1], send_sem=asend, recv_sem=arecv, device_id=partner,
         device_id_type=MESH,
     ).wait_recv()
-    x_all = xs[...].reshape(NZ * 16, 128)
+    x_rows = jnp.concatenate([xs[k].astype(F32) for k in range(NZ)], axis=0).astype(BF16)
+    to_row = iota((128, 32), 0)
+    from_row = iota((128, 32), 1)
+    packed_row = lax.rem(to_row, 16)
+    spread = one_hot((to_row // 16 == from_row // 4) & (packed_row // CB == lax.rem(from_row, 4)) & (packed_row < 3 * CB))
+    x_all = jnp.concatenate([dot(spread, x_rows[i * 32 : (i + 1) * 32]) for i in range(4)], axis=0).astype(BF16)
     block_of = lax.rem(lax.rem(iota((NZ * 16, 128), 0), 16), CB)
     zero = jnp.zeros_like(x_all)
     stacked = jnp.concatenate([jnp.where(block_of == cb, x_all, zero) for cb in range(CB)], axis=1)
@@ -458,6 +534,22 @@
     arranged = sum(dot(one_hot((lax.rem(trow, 2) == k) & (tcol == want)), totals[k]) for k in range(2))
     for j in range(3):
         mixed_o[j] = arranged[j * 16 : (j + 1) * 16].astype(BF16)
+
+    @pl.when(o + 8 < NZ)
+    def _():
+        def left_right(slot, _):
+            copy_slice(rel0.at[slot], rel0.at[slot], r0send.at[slot], arecv, o + 8).wait_send()
+            return 0
+
+        lax.fori_loop(jnp.maximum(8 - o, 0), 8, left_right, 0)
+
+    @pl.when(o + 24 < NZ)
+    def _():
+        def left_left(slot, _):
+            copy_slice(rel1.at[slot], rel1.at[slot], r1send.at[slot], arecv, o + 24).wait_send()
+            return 0
+
+        lax.fori_loop(0, 7, left_left, 0)
 
     for cp in shares:
         cp.wait_send()
@@ -534,8 +626,8 @@
             pltpu.VMEM((64, channels), BF16),
             pltpu.VMEM((64, channels), BF16),
             pltpu.VMEM((CB * 128, BLK), BF16),
-            pltpu.VMEM((NZ, 16, 128), BF16),
-            pltpu.VMEM((NZ, 16, 128), BF16),
+            pltpu.VMEM((NZ, 4, 128), BF16),
+            pltpu.VMEM((NZ, 4, 128), BF16),
             pltpu.VMEM((NZ, 16, BLK), BF16),
             pltpu.VMEM((8, 4, 16, BLK), BF16),
             pltpu.VMEM((7, 16, BLK), BF16),
@@ -559,6 +651,13 @@
             dma,
             dma((7,)),
             dma((7,)),
+            pltpu.VMEM((8, 4, 128), BF16),
+            pltpu.VMEM((7, 4, 128), BF16),
+            dma((8,)),
+            dma((8,)),
+            dma((7,)),
+            dma((7,)),
+            pltpu.SemaphoreType.REGULAR((NZ,)),
         ],
         compiler_params=pltpu.CompilerParams(
             collective_id=0, has_side_effects=True, vmem_limit_bytes=56 * 1024 * 1024

time: 130 us -> 118 us (0.908)
  Pallas kernels: 129 us -> 116 us
    pallas_call x1, Pallas kernels: 127 us -> 114 us  [local(): pl.pallas_call(kernel, name='mixer', out_shape=(pltpu.VMEM((3, 16, 64), B...]
where the time goes in v3:
time: 118 us; the launch traced here: 117 us
  Pallas kernels  116 us (98%)
  between operations  1.29 us (1%)
    pallas_call x1, Pallas kernels, local(): pl.pallas_call(kernel, name='mixer', out_shape=(pltpu.VMEM((3, 16, 64), B...  114 us

profile of v3, /device:TPU:33, one launch (start us, length us, event | category | flops | bytes accessed | tf_op | source)
XLA Modules:
  0.0 117.3 jit_solution(6464071175496209621)
XLA Ops:
  1.3 114.3 %mixer.1 = (bf16[3,16,64]{2,1,0:T(8,128)(2,1)S(1)}, f32[3,2048,64]{2,1,0:T(8,128)S(1)}, bf16[6,2,1152]{2,1,0:T(2,128)(2,1)S(1)}) custom-call(bf16[1,3,4096]{2,1,0:T(4,128)(2,1)} %tok_h.1, f32[1,4096]{1,0:T(1,128)} %bitcast.15, bf16[64,2048]{1,0:T(8,128)(2,1)} %wh_h.1, bf16[64,2048]{1,0:T(8,128)(2,1)} %wg_h.1, bf16[64,128]{1,0:T(8,128)(2,1)} %wi_h.1, ...), custom_call_target="tpu_custom_call" | custom-call | tf_op jit(solution)/shard_map/mixer/pallas_call | solution.py:604
  115.6 1.7 %store.1 = (bf16[3,16,64]{2,1,0:T(8,128)(2,1)}, f32[3,2048,64]{2,1,0:T(8,128)}, bf16[6,2,1152]{2,1,0:T(2,128)(2,1)}) custom-call(bf16[3,16,64]{2,1,0:T(8,128)(2,1)S(1)} %get-tuple-element.9.mixed, f32[3,2048,64]{2,1,0:T(8,128)S(1)} %get-tuple-element.10.states, bf16[6,2,1152]{2,1,0:T(2,128)(2,1)S(1)} %get-tuple-element.11.tail), custom_call_target="tpu_custom_call" | custom-call | tf_op jit(solution)/shard_map/store/pallas_call | solution.py:684

commit v4 on v3

--- a/solution.py
+++ b/solution.py
@@ -16,6 +16,9 @@
 KV = ("z", "c")
 GRP_KV = ("grp", "z", "c")
 
+STAGES = (0, 16, 24, 32)
+LAST = 28
+CLOSE = 26
 NZ = 32
 BLK = 896
 CB = 5
@@ -67,11 +70,11 @@
 
 
 def kernel(
-    tok_h, ins_h, wh_h, wg_h, wi_h, wr_h, ws_h, bias_h, ldr_h, dpw_h, tap_h, hist_h, st_h, acc_s, ped_h, gns_h, wo_h,
+    tok_h, ins_h, wh_h, wg_h, wi_h, wr_h, ws_h, bias_h, ldr_h, dpw_h, tap_h, hist_h, st_h, acc_h, ped_h, gns_h, wo_h,
     mixed_o, snew, tail_o,
     tok, ins, ws, bias, ldr, dpw, tap, hist, st, ped, gns, wo, wop,
     w2, nst, xs, part, mem, cout, cin, gath, gown, fin, fst, s0cat,
-    lsem, wsend, wrecv, asend, arecv, msend, mrecv, csend, crecv, gsend, grecv, nrecv, fsend, frecv, rel0, rel1, r0send, r0recv, r1send, r1recv, may,
+    lsem, wsend, wrecv, asend, arecv, msend, mrecv, csend, crecv, gsend, grecv, nrecv, fsend, frecv, rel0, rel1, r0send, r0recv, r1send, r1recv, may, acc_s, rel2, r2send, r2recv,
 ):
     z = lax.axis_index("z")
     c = lax.axis_index("c")
@@ -83,12 +86,18 @@
     def at(offset):
         return lax.rem(z + (offset + NZ) % NZ, NZ)
 
+    def place_of(offset):
+        return lax.rem(o + (offset + NZ) % NZ, NZ)
+
     def chip(place):
         return lax.rem(place + 1, NZ)
 
+    def stage_of(place):
+        return jnp.where(place < STAGES[1], 0, jnp.where(place < STAGES[2], 1, 2))
+
     pairs = [
         (tok_h.at[0], tok), (ins_h, ins), (ws_h, ws), (bias_h, bias), (ldr_h, ldr), (dpw_h, dpw), (tap_h, tap),
-        (hist_h.at[0], hist), (ped_h, ped), (gns_h, gns), (st_h, st), (wo_h, wo),
+        (hist_h.at[0], hist), (ped_h, ped), (gns_h, gns), (st_h, st), (wo_h, wo), (acc_h, acc_s),
     ]
     loads = [pltpu.make_async_copy(src, dst, lsem.at[i]) for i, (src, dst) in enumerate(pairs)]
     sources = (wh_h, wg_h, wi_h, wr_h)
@@ -122,7 +131,10 @@
     def tell(k, _):
         to = chip(o - k)
 
-        @pl.when((k <= 8) | (k >= 24) | ((k >= 17) & (o < 24)))
+        usual = (k <= 8) | (k >= 24) | ((k >= 17) & (o < 24))
+        last = (k == LAST) | (k <= o - CLOSE)
+
+        @pl.when(((o < LAST) & usual) | ((o >= LAST) & last))
         def _():
             pl.semaphore_signal(may.at[o], inc=1, device_id={"z": to}, device_id_type=MESH)
 
@@ -146,7 +158,7 @@
         )
 
     def direct_slice(to):
-        copy_slice(nst.at[chip(to)], xs.at[z], asend, arecv, to).start()
+        copy_slice(nst.at[chip(to)], xs.at[o], asend, arecv.at[stage_of(o)], to).start()
 
     def send_back(to, _):
         direct_slice(to)
@@ -159,8 +171,17 @@
         copy_slice(nst.at[chip(to)], rel1.at[o - relay - 1], asend, r1recv.at[o - relay - 1], relay).start()
         return 0
 
-    lax.fori_loop(jnp.maximum(o + 17, 24), jnp.minimum(o + 24, NZ), send_by_first, 0)
-    xs[z] = nst[z]
+    lax.fori_loop(jnp.maximum(o + 17, 24), jnp.minimum(o + 24, LAST), send_by_first, 0)
+
+    def send_by_wrap(relay, _):
+        copy_slice(nst.at[chip(relay + LAST)], rel2.at[o], asend, r2recv.at[o], relay).start()
+        return 0
+
+    @pl.when(o < CLOSE)
+    def _():
+        lax.fori_loop(0, jnp.minimum(o, NZ - LAST), send_by_wrap, 0)
+
+    xs[o] = nst[z]
 
     partner = {"c": 1 - c}
     shares = []
@@ -241,24 +262,79 @@
     context = jnp.where(accepted == 1, kept[1:4], jnp.where(accepted == 2, kept[2:5], kept[3:6]))
     context = jnp.concatenate([context, jnp.zeros((5, context.shape[1]), F32)], axis=0)
 
+    to_row = iota((128, 32), 0)
+    from_row = iota((128, 32), 1)
+    packed_row = lax.rem(to_row, 16)
+    spread = one_hot((to_row // 16 == from_row // 4) & (packed_row // CB == lax.rem(from_row, 4)) & (packed_row < 3 * CB))
+
+    def member(delta, hop, head, slot, when):
+        dest = place_of(delta)
+
+        @pl.when(when(stage_of(dest), o + hop < 0))
+        def _():
+            pltpu.make_async_remote_copy(
+                src_ref=part.at[dest], dst_ref=mem.at[head // 4, slot], send_sem=msend, recv_sem=mrecv.at[head // 4],
+                device_id={"z": at(hop)}, device_id_type=MESH,
+            ).start()
+
+    def members(head, when):
+        member((head + 1) % NZ, 1, head, 0, when)
+        member((head - 1) % NZ, -1, head, 1, when)
+        if head < 16:
+            member(head + 2, 2, head, 2, when)
+        if head > 16:
+            member(head - 2, -2, head, 2, when)
+        if head == 0:
+            member(NZ - 2, -2, head, 3, when)
+
+    def arrived(stage):
+        first, last = STAGES[stage], STAGES[stage + 1]
+
+        def wait(count):
+            pltpu.make_async_remote_copy(
+                src_ref=xs.at[0:count], dst_ref=xs.at[0:count], send_sem=asend, recv_sem=arecv.at[stage],
+                device_id=partner, device_id_type=MESH,
+            ).wait_recv()
+
+        @pl.when(stage_of(o) == stage)
+        def _():
+            wait(last - first - 1)
+
+        @pl.when(stage_of(o) != stage)
+        def _():
+            wait(last - first)
+
+    def multiply(stage):
+        first, last = STAGES[stage], STAGES[stage + 1]
+        rows = (last - first) * 16
+        x_rows = jnp.concatenate([xs[k].astype(F32) for k in range(first, last)], axis=0).astype(BF16)
+        x_all = jnp.concatenate([dot(spread, x_rows[i : i + 32]) for i in range(0, x_rows.shape[0], 32)], axis=0)
+        x_all = x_all.astype(BF16)
+        block_of = lax.rem(lax.rem(iota((rows, 128), 0), 16), CB)
+        zero = jnp.zeros_like(x_all)
+        stacked = jnp.concatenate([jnp.where(block_of == cb, x_all, zero) for cb in range(CB)], axis=1)
+        for n0, n1 in ((0, 256), (256, 512), (512, 768), (768, 896)):
+            part[first:last, :, n0:n1] = dot(stacked, w2[:, n0:n1]).astype(BF16).reshape(last - first, 16, n1 - n0)
+
     def send_near(to, _):
         pl.semaphore_wait(may.at[to], 1)
         direct_slice(to)
 
-        @pl.when(to + 8 < NZ)
+        @pl.when(to + 8 < LAST)
         def _():
             slot = o - to + 8
             copy_slice(nst.at[chip(to + 8)], rel0.at[slot], asend, r0recv.at[slot], to).start()
 
         return 0
 
-    lax.fori_loop(o + 1, jnp.minimum(o + 9, NZ), send_near, 0)
+    lax.fori_loop(o + 1, jnp.minimum(o + 9, jnp.where(o < CLOSE, LAST, NZ)), send_near, 0)
+    lax.fori_loop(o + 1, NZ - LAST, send_by_wrap, 0)
 
     def pass_on(rel, slot, source, sems, recv, to):
         copy_slice(rel.at[slot], rel.at[slot], asend, recv.at[slot], to).wait_recv()
-        copy_slice(rel.at[slot], xs.at[chip(source)], sems.at[slot], arecv, to).start()
-
-    @pl.when(o + 8 < NZ)
+        copy_slice(rel.at[slot], xs.at[source], sems.at[slot], arecv.at[stage_of(source)], to).start()
+
+    @pl.when(o + 8 < LAST)
     def _():
         def pass_right(slot, _):
             pass_on(rel0, slot, o - 8 + slot, r0send, r0recv, o + 8)
@@ -271,9 +347,16 @@
         direct_slice(to)
         return 0
 
-    lax.fori_loop(o + 17, 24, send_far, 0)
-
-    @pl.when(o + 24 < NZ)
+    lax.fori_loop(o + 17, STAGES[2], send_far, 0)
+
+    for cp in shares:
+        cp.wait_recv()
+    arrived(0)
+    multiply(0)
+    for head in (16, 12, 20, 8, 24, 4, 28, 0):
+        members(head, lambda stage, edge: (o < STAGES[2]) & (stage == 0) & ~edge)
+
+    @pl.when(o + 24 < LAST)
     def _():
         send_far(o + 24, 0)
 
@@ -283,41 +366,32 @@
 
         lax.fori_loop(0, 7, pass_left, 0)
 
-    lax.fori_loop(o + 25, NZ, send_far, 0)
-
-    for cp in shares:
-        cp.wait_recv()
-    pltpu.make_async_remote_copy(
-        src_ref=nst.at[0 : NZ - 1], dst_ref=xs.at[0 : NZ - 1], send_sem=asend, recv_sem=arecv, device_id=partner,
-        device_id_type=MESH,
-    ).wait_recv()
-    x_rows = jnp.concatenate([xs[k].astype(F32) for k in range(NZ)], axis=0).astype(BF16)
-    to_row = iota((128, 32), 0)
-    from_row = iota((128, 32), 1)
-    packed_row = lax.rem(to_row, 16)
-    spread = one_hot((to_row // 16 == from_row // 4) & (packed_row // CB == lax.rem(from_row, 4)) & (packed_row < 3 * CB))
-    x_all = jnp.concatenate([dot(spread, x_rows[i * 32 : (i + 1) * 32]) for i in range(4)], axis=0).astype(BF16)
-    block_of = lax.rem(lax.rem(iota((NZ * 16, 128), 0), 16), CB)
-    zero = jnp.zeros_like(x_all)
-    stacked = jnp.concatenate([jnp.where(block_of == cb, x_all, zero) for cb in range(CB)], axis=1)
-    for n0, n1 in ((0, 256), (256, 512), (512, 768), (768, 896)):
-        part[:, :, n0:n1] = dot(stacked, w2[:, n0:n1]).astype(BF16).reshape(NZ, 16, n1 - n0)
-
-    def member(delta, hop, head, slot):
-        pltpu.make_async_remote_copy(
-            src_ref=part.at[at(delta)], dst_ref=mem.at[head // 4, slot], send_sem=msend, recv_sem=mrecv.at[head // 4],
-            device_id={"z": at(hop)}, device_id_type=MESH,
-        ).start()
-
-    def members(head):
-        member((head + 1) % NZ, 1, head, 0)
-        member((head - 1) % NZ, -1, head, 1)
-        if head < 16:
-            member(head + 2, 2, head, 2)
-        if head > 16:
-            member(head - 2, -2, head, 2)
-        if head == 0:
-            member(NZ - 2, -2, head, 3)
+    lax.fori_loop(o + 25, LAST, send_far, 0)
+
+    @pl.when(o + LAST < NZ)
+    def _():
+        send_far(o + LAST, 0)
+
+        def pass_wrap(slot, _):
+            @pl.when(slot != o)
+            def _():
+                pass_on(rel2, slot, slot, r2send, r2recv, o + LAST)
+
+            return 0
+
+        lax.fori_loop(0, CLOSE, pass_wrap, 0)
+
+
+    arrived(1)
+    multiply(1)
+    for head in (16, 12, 20, 8, 24, 4, 28, 0):
+        members(head, lambda stage, edge: (o < STAGES[2]) & (stage == 1) & ~edge)
+
+    arrived(2)
+    multiply(2)
+
+    def late(stage, edge):
+        return (o >= STAGES[2]) | (stage == 2) | edge
 
     def quad(head):
         count = {0: 4, 16: 2}.get(head, 3)
@@ -325,7 +399,7 @@
             src_ref=mem.at[head // 4, 0:count], dst_ref=mem.at[head // 4, 0:count], send_sem=msend,
             recv_sem=mrecv.at[head // 4], device_id=partner, device_id_type=MESH,
         ).wait_recv()
-        total = part[at(head)].astype(F32)
+        total = part[place_of(head)].astype(F32)
         for slot in range(count):
             total += mem[head // 4, slot].astype(F32)
         return total
@@ -339,13 +413,13 @@
     right = [chain(i, 4) for i in range(4)]
     left = [chain(4 + i, -4) for i in range(3)]
     for head in (16, 12, 20):
-        members(head)
+        members(head, late)
     cout[0] = quad(16).astype(BF16)
     right[0].start()
     cout[4] = quad(20).astype(BF16)
     left[0].start()
     for head in (8, 24):
-        members(head)
+        members(head, late)
     total = quad(12)
     right[0].wait_recv()
     cout[1] = (total + cin[0].astype(F32)).astype(BF16)
@@ -355,7 +429,7 @@
     cout[5] = (total + cin[4].astype(F32)).astype(BF16)
     left[1].start()
     for head in (4, 28):
-        members(head)
+        members(head, late)
     total = quad(8)
     right[1].wait_recv()
     cout[2] = (total + cin[1].astype(F32)).astype(BF16)
@@ -364,7 +438,7 @@
     left[1].wait_recv()
     cout[6] = (total + cin[5].astype(F32)).astype(BF16)
     left[2].start()
-    members(0)
+    members(0, late)
     total = quad(4)
     right[2].wait_recv()
     cout[3] = (total + cin[2].astype(F32)).astype(BF16)
@@ -535,18 +609,29 @@
     for j in range(3):
         mixed_o[j] = arranged[j * 16 : (j + 1) * 16].astype(BF16)
 
-    @pl.when(o + 8 < NZ)
+    @pl.when(o + 8 < LAST)
     def _():
         def left_right(slot, _):
-            copy_slice(rel0.at[slot], rel0.at[slot], r0send.at[slot], arecv, o + 8).wait_send()
+            copy_slice(rel0.at[slot], rel0.at[slot], r0send.at[slot], arecv.at[0], o + 8).wait_send()
             return 0
 
         lax.fori_loop(jnp.maximum(8 - o, 0), 8, left_right, 0)
 
-    @pl.when(o + 24 < NZ)
+    @pl.when(o + LAST < NZ)
+    def _():
+        def left_wrap(slot, _):
+            @pl.when(slot != o)
+            def _():
+                copy_slice(rel2.at[slot], rel2.at[slot], r2send.at[slot], arecv.at[0], o + LAST).wait_send()
+
+            return 0
+
+        lax.fori_loop(0, CLOSE, left_wrap, 0)
+
+    @pl.when(o + 24 < LAST)
     def _():
         def left_left(slot, _):
-            copy_slice(rel1.at[slot], rel1.at[slot], r1send.at[slot], arecv, o + 24).wait_send()
+            copy_slice(rel1.at[slot], rel1.at[slot], r1send.at[slot], arecv.at[0], o + 24).wait_send()
             return 0
 
         lax.fori_loop(0, 7, left_left, 0)
@@ -559,7 +644,7 @@
         cp.wait_send()
     for ref, count, sem in ((xs, NZ - 1, asend), (part, 24, msend), (gath, NZ - 1, gsend)):
         pltpu.make_async_remote_copy(
-            src_ref=ref.at[0:count], dst_ref=ref.at[0:count], send_sem=sem, recv_sem=arecv, device_id=partner,
+            src_ref=ref.at[0:count], dst_ref=ref.at[0:count], send_sem=sem, recv_sem=arecv.at[0], device_id=partner,
             device_id_type=MESH,
         ).wait_send()
 
@@ -599,7 +684,6 @@
     channels = heads * 64
     dma = pltpu.SemaphoreType.DMA
     any_space = pl.BlockSpec(memory_space=pl.ANY)
-    smem = pl.BlockSpec(memory_space=pltpu.SMEM)
     vmem = pl.BlockSpec(memory_space=pltpu.VMEM)
     mixed, states, tail = pl.pallas_call(
         kernel,
@@ -609,7 +693,7 @@
             pltpu.VMEM((3, channels, 64), F32),
             pltpu.VMEM((6, 2, 1152), BF16),
         ),
-        in_specs=[any_space] * 13 + [smem] + [any_space] * 3,
+        in_specs=[any_space] * 17,
         out_specs=(vmem, vmem, vmem),
         scratch_shapes=[
             pltpu.VMEM((3, width), BF16),
@@ -637,11 +721,11 @@
             pltpu.VMEM((2, 4, 32, 64), BF16),
             pltpu.VMEM((2, 4, 32, 64), BF16),
             pltpu.VMEM((channels, 128), BF16),
-            dma((12 + len(PIECES),)),
+            dma((13 + len(PIECES),)),
             dma((len(PIECES) + 1,)),
             dma((len(PIECES) + 1,)),
             dma,
-            dma,
+            dma((3,)),
             dma,
             dma((8,)),
             dma((7,)),
@@ -658,6 +742,10 @@
             dma((7,)),
             dma((7,)),
             pltpu.SemaphoreType.REGULAR((NZ,)),
+            pltpu.SMEM((1,), jnp.int32),
+            pltpu.VMEM((CLOSE, 4, 128), BF16),
+            dma((CLOSE,)),
+            dma((CLOSE,)),
         ],
         compiler_params=pltpu.CompilerParams(
             collective_id=0, has_side_effects=True, vmem_limit_bytes=56 * 1024 * 1024

time: 118 us -> 116 us (0.983)
  Pallas kernels: 116 us -> 114 us
    pallas_call x1, Pallas kernels: 114 us -> 113 us  [local(): pl.pallas_call(kernel, name='mixer', out_shape=(pltpu.VMEM((3, 16, 64), B...]
where the time goes in v4:
time: 116 us
  Pallas kernels  114 us (98%)
  between operations  1.29 us (1%)
    pallas_call x1, Pallas kernels, local(): pl.pallas_call(kernel, name='mixer', out_shape=(pltpu.VMEM((3, 16, 64), B...  113 us

profile of v4, /device:TPU:33, one launch (start us, length us, event | category | flops | bytes accessed | tf_op | source)
XLA Modules:
  0.0 115.6 jit_solution(8590239190410981928)
XLA Ops:
  1.3 112.6 %mixer.1 = (bf16[3,16,64]{2,1,0:T(8,128)(2,1)S(1)}, f32[3,2048,64]{2,1,0:T(8,128)S(1)}, bf16[6,2,1152]{2,1,0:T(2,128)(2,1)S(1)}) custom-call(bf16[1,3,4096]{2,1,0:T(4,128)(2,1)} %tok_h.1, f32[1,4096]{1,0:T(1,128)} %bitcast.15, bf16[64,2048]{1,0:T(8,128)(2,1)} %wh_h.1, bf16[64,2048]{1,0:T(8,128)(2,1)} %wg_h.1, bf16[64,128]{1,0:T(8,128)(2,1)} %wi_h.1, ...), custom_call_target="tpu_custom_call" | custom-call | tf_op jit(solution)/shard_map/mixer/pallas_call | solution.py:688
  113.9 1.7 %store.1 = (bf16[3,16,64]{2,1,0:T(8,128)(2,1)}, f32[3,2048,64]{2,1,0:T(8,128)}, bf16[6,2,1152]{2,1,0:T(2,128)(2,1)}) custom-call(bf16[3,16,64]{2,1,0:T(8,128)(2,1)S(1)} %get-tuple-element.9.mixed, f32[3,2048,64]{2,1,0:T(8,128)S(1)} %get-tuple-element.10.states, bf16[6,2,1152]{2,1,0:T(2,128)(2,1)S(1)} %get-tuple-element.11.tail), custom_call_target="tpu_custom_call" | custom-call | tf_op jit(solution)/shard_map/store/pallas_call | solution.py:772

commit v5 on v4

--- a/solution.py
+++ b/solution.py
@@ -19,6 +19,7 @@
 STAGES = (0, 16, 24, 32)
 LAST = 28
 CLOSE = 26
+FIRST = 8
 NZ = 32
 BLK = 896
 CB = 5
@@ -551,13 +552,67 @@
     for i in range(6):
         tail_o[i] = jnp.concatenate([groups[0][i : i + 1], groups[1][i : i + 1]], axis=0).astype(BF16)
 
-    for k in (1, 7, 2, 6, 3, 5, 4):
-        slot = at(-4 * k)
+    @pl.when(o + 8 < LAST)
+    def _():
+        def left_right(slot, _):
+            copy_slice(rel0.at[slot], rel0.at[slot], r0send.at[slot], arecv.at[0], o + 8).wait_send()
+            return 0
+
+        lax.fori_loop(jnp.maximum(8 - o, 0), 8, left_right, 0)
+
+    @pl.when(o + LAST < NZ)
+    def _():
+        def left_wrap(slot, _):
+            @pl.when(slot != o)
+            def _():
+                copy_slice(rel2.at[slot], rel2.at[slot], r2send.at[slot], arecv.at[0], o + LAST).wait_send()
+
+            return 0
+
+        lax.fori_loop(0, CLOSE, left_wrap, 0)
+
+    @pl.when(o + 24 < LAST)
+    def _():
+        def left_left(slot, _):
+            copy_slice(rel1.at[slot], rel1.at[slot], r1send.at[slot], arecv.at[0], o + 24).wait_send()
+            return 0
+
+        lax.fori_loop(0, 7, left_left, 0)
+
+    for cp in shares:
+        cp.wait_send()
+    for cp in right + left:
+        cp.wait_send()
+    for ref, count, sem in ((xs, NZ - 1, asend), (part, 24, msend)):
         pltpu.make_async_remote_copy(
-            src_ref=gown, dst_ref=gath.at[slot], send_sem=gsend, recv_sem=grecv.at[k], device_id=partner, device_id_type=MESH
-        ).wait_recv()
-        for hop in (-1, 1) + ((2,) if k < 4 else (-2,) if k > 4 else ()):
-            share(gath.at[slot], slot, hop, nrecv)
+            src_ref=ref.at[0:count], dst_ref=ref.at[0:count], send_sem=sem, recv_sem=arecv.at[0], device_id=partner,
+            device_id_type=MESH,
+        ).wait_send()
+
+    def pass_gated(i, _):
+        source = lax.rem(FIRST + lax.rem(z, 4) + 4 * i, NZ)
+        k = lax.rem(z - source + NZ, NZ) // 4
+
+        @pl.when(source != z)
+        def _():
+            pltpu.make_async_remote_copy(
+                src_ref=gown, dst_ref=gath.at[source], send_sem=gsend, recv_sem=grecv.at[k], device_id=partner,
+                device_id_type=MESH,
+            ).wait_recv()
+            share(gath.at[source], source, -1, nrecv)
+            share(gath.at[source], source, 1, nrecv)
+
+            @pl.when(k < 4)
+            def _():
+                share(gath.at[source], source, 2, nrecv)
+
+            @pl.when(k > 4)
+            def _():
+                share(gath.at[source], source, -2, nrecv)
+
+        return 0
+
+    lax.fori_loop(0, NZ // 4, pass_gated, 0)
     pltpu.make_async_remote_copy(
         src_ref=gath.at[0:24], dst_ref=gath.at[0:24], send_sem=gsend, recv_sem=nrecv, device_id=partner, device_id_type=MESH
     ).wait_recv()
@@ -609,44 +664,12 @@
     for j in range(3):
         mixed_o[j] = arranged[j * 16 : (j + 1) * 16].astype(BF16)
 
-    @pl.when(o + 8 < LAST)
-    def _():
-        def left_right(slot, _):
-            copy_slice(rel0.at[slot], rel0.at[slot], r0send.at[slot], arecv.at[0], o + 8).wait_send()
-            return 0
-
-        lax.fori_loop(jnp.maximum(8 - o, 0), 8, left_right, 0)
-
-    @pl.when(o + LAST < NZ)
-    def _():
-        def left_wrap(slot, _):
-            @pl.when(slot != o)
-            def _():
-                copy_slice(rel2.at[slot], rel2.at[slot], r2send.at[slot], arecv.at[0], o + LAST).wait_send()
-
-            return 0
-
-        lax.fori_loop(0, CLOSE, left_wrap, 0)
-
-    @pl.when(o + 24 < LAST)
-    def _():
-        def left_left(slot, _):
-            copy_slice(rel1.at[slot], rel1.at[slot], r1send.at[slot], arecv.at[0], o + 24).wait_send()
-            return 0
-
-        lax.fori_loop(0, 7, left_left, 0)
-
-    for cp in shares:
-        cp.wait_send()
-    for cp in right + left:
-        cp.wait_send()
     for cp in finals:
         cp.wait_send()
-    for ref, count, sem in ((xs, NZ - 1, asend), (part, 24, msend), (gath, NZ - 1, gsend)):
-        pltpu.make_async_remote_copy(
-            src_ref=ref.at[0:count], dst_ref=ref.at[0:count], send_sem=sem, recv_sem=arecv.at[0], device_id=partner,
-            device_id_type=MESH,
-        ).wait_send()
+    pltpu.make_async_remote_copy(
+        src_ref=gath.at[0 : NZ - 1], dst_ref=gath.at[0 : NZ - 1], send_sem=gsend, recv_sem=nrecv, device_id=partner,
+        device_id_type=MESH,
+    ).wait_send()
 
 
 def store(mixed, states, tail, mixed_o, states_o, tail_o, sem):

time: 116 us -> 115 us (level)
  no operation moved by 1% of the time
where the time goes in v5:
time: 115 us
  Pallas kernels  114 us (99%)
  between operations  1.29 us (1%)
    pallas_call x1, Pallas kernels, local(): pl.pallas_call(kernel, name='mixer', out_shape=(pltpu.VMEM((3, 16, 64), B...  112 us

profile of v5, /device:TPU:33, one launch (start us, length us, event | category | flops | bytes accessed | tf_op | source)
XLA Modules:
  0.0 115.0 jit_solution(4706953271076366096)
XLA Ops:
  1.3 112.0 %mixer.1 = (bf16[3,16,64]{2,1,0:T(8,128)(2,1)S(1)}, f32[3,2048,64]{2,1,0:T(8,128)S(1)}, bf16[6,2,1152]{2,1,0:T(2,128)(2,1)S(1)}) custom-call(bf16[1,3,4096]{2,1,0:T(4,128)(2,1)} %tok_h.1, f32[1,4096]{1,0:T(1,128)} %bitcast.15, bf16[64,2048]{1,0:T(8,128)(2,1)} %wh_h.1, bf16[64,2048]{1,0:T(8,128)(2,1)} %wg_h.1, bf16[64,128]{1,0:T(8,128)(2,1)} %wi_h.1, ...), custom_call_target="tpu_custom_call" | custom-call | tf_op jit(solution)/shard_map/mixer/pallas_call | solution.py:711
  113.3 1.7 %store.1 = (bf16[3,16,64]{2,1,0:T(8,128)(2,1)}, f32[3,2048,64]{2,1,0:T(8,128)}, bf16[6,2,1152]{2,1,0:T(2,128)(2,1)}) custom-call(bf16[3,16,64]{2,1,0:T(8,128)(2,1)S(1)} %get-tuple-element.9.mixed, f32[3,2048,64]{2,1,0:T(8,128)S(1)} %get-tuple-element.10.states, bf16[6,2,1152]{2,1,0:T(2,128)(2,1)S(1)} %get-tuple-element.11.tail), custom_call_target="tpu_custom_call" | custom-call | tf_op jit(solution)/shard_map/store/pallas_call | solution.py:795
